TPU v7x, 768 devices: a whole 4x8x12 slice. The times are simulated.
768 devices in a mesh: sp: 384 (over z, y, x), tp: 2 (over core).
Axes of the slice: x: 4, y: 8, z: 12, core: 2. Of those that a mesh axis runs over, the one named last changes fastest.
Arguments:
- value_in: bfloat16 [98304, 2048], P('sp', 'tp'), may hold values from -25 to 25, as said below
- gate_in: bfloat16 [98304, 2048], P('sp', 'tp'), may hold values from -6 to 6
- taps: float32 [31, 2048], P(None, 'tp'), may hold values from -1 to 1
- gain: float32 [2048], P('tp'), may hold values from 0.1 to 1.9
- shift: float32 [2048], P('tp'), may hold values from -3 to 3
- w_out: bfloat16 [2048, 2048], P('tp'), may hold values from -0.125 to 0.125
- grad_out: bfloat16 [98304, 2048], P('sp'), may hold values from -6 to 6
Outputs:
- d_value: bfloat16 [98304, 2048], P('sp', 'tp')
- d_gate: bfloat16 [98304, 2048], P('sp', 'tp')
- d_taps: float32 [31, 2048], P(None, 'tp')
- d_gain: float32 [2048], P('tp')
- d_shift: float32 [2048], P('tp')
Inputs may be any that keep to these rules, and one draw needn't show every extreme that they name: `value_in`: channel blocks of different magnitude.
All inputs are finite; a program needn't handle non-finite values.
Results may differ from a plain program's by a relative error of at most 0.007.
Values may be sent and summed in bfloat16 or wider, within the bound.
A program may use at most 64 MiB of HBM per device.

v0:
```python
import math

import jax
import jax.numpy as jnp
from jax import lax
from jax.sharding import Mesh
from jax.sharding import PartitionSpec as P

SP = ("sp_0", "sp_1", "sp_2")


EPS = 1e-05


def from_everyone(value, axis):
    peers = lax.axis_size(axis)
    return lax.all_to_all(
        jnp.broadcast_to(value[None], (peers, *value.shape)), axis, 0, 0, tiled=True
    )


def of_everyone(value, axis):
    everything = from_everyone(value, axis)
    return jnp.sum(everything, axis=0)


def together(arrays, axis):
    ends = [0]
    for a in arrays:
        ends.append(ends[-1] + a.size)
    running = of_everyone(jnp.concatenate([a.ravel() for a in arrays]), axis)
    return tuple((running[b:e].reshape(a.shape) for a, b, e in zip(arrays, ends, ends[1:])))


def with_halo(block, sides, width):
    for axis, dim in sides:
        count = lax.axis_size(axis)
        forward = [(i, i + 1) for i in range(count - 1)]
        backward = [(target, source) for source, target in forward]
        low = lax.ppermute(
            lax.slice_in_dim(block, block.shape[dim] - width, None, axis=dim), axis, forward
        )
        high = lax.ppermute(lax.slice_in_dim(block, 0, width, axis=dim), axis, backward)
        block = jnp.concatenate([low, block, high], axis=dim)
    return block


def by_axis(value, axes):
    for axis in axes:
        value = lax.psum(value, axis)
    return value


def gated_rows(value_rows, gate_rows):
    gate_sig = jax.nn.sigmoid(gate_rows.astype(jnp.float32))
    return ((value_rows.astype(jnp.float32) * gate_sig).astype(jnp.bfloat16), gate_sig)


def convolve(window, taps, count):
    wide = window.astype(jnp.float32)
    total = jnp.zeros((count, wide.shape[1]), jnp.float32)
    for offset in range(taps.shape[0]):
        total = total + taps[offset] * wide[offset : offset + count]
    return total


def norm_backward(conv_out, grad_rows, gain, shift, w_out, width):
    sums, squares = lax.psum((jnp.sum(conv_out, 1), jnp.sum(conv_out * conv_out, 1)), "tp")
    mean = sums / width
    var = squares / width - mean * mean
    inv = lax.rsqrt(var + EPS)
    normed = (conv_out - mean[:, None]) * inv[:, None]
    pre = normed * gain + shift
    grad_mix = lax.dot_general(
        grad_rows, w_out, (((1,), (1,)), ((), ())), preferred_element_type=jnp.float32
    )
    sig = jax.nn.sigmoid(pre)
    grad_pre = grad_mix * sig * (1.0 + pre * (1.0 - sig))
    grad_normed = grad_pre * gain
    first, second = together((jnp.sum(grad_normed, 1), jnp.sum(grad_normed * normed, 1)), "tp")
    grad_conv = inv[:, None] * (
        grad_normed - first[:, None] / width - normed * second[:, None] / width
    )
    return (grad_conv, grad_pre, normed)


def shards(value_in, gate_in, taps, gain, shift, w_out, grad_out):
    half = taps.shape[0] // 2
    kernel = taps.shape[0]
    rows = value_in.shape[0]
    width = value_in.shape[1] * lax.axis_size("tp")
    total = rows * lax.axis_size(SP)
    value_ext, gate_ext, cotan_ext = (
        with_halo(value_in, ((SP, 0),), 2 * half),
        with_halo(gate_in, ((SP, 0),), 2 * half),
        with_halo(grad_out, ((SP, 0),), 2 * half),
    )
    gated_big, sig_big = gated_rows(value_ext, gate_ext)
    conv_ext = convolve(gated_big, taps, rows + 2 * half)
    grad_wide, pre_ext, normed_ext = norm_backward(
        conv_ext, cotan_ext[half : 3 * half + rows], gain, shift, w_out, width
    )
    gated_wide = gated_big[half : 3 * half + rows]
    gate_sig = sig_big[2 * half : 2 * half + rows]
    grad_pre = pre_ext[half : half + rows]
    normed = normed_ext[half : half + rows]
    own_grad = grad_wide[half : half + rows]
    gated_float = gated_wide.astype(jnp.float32)
    grad_gated = jnp.zeros((rows, own_grad.shape[1]), jnp.float32)
    for offset in range(kernel):
        grad_gated = (
            grad_gated + taps[offset] * grad_wide[2 * half - offset : 2 * half - offset + rows]
        )
    tap_terms = jnp.stack(
        [jnp.sum(own_grad * gated_float[offset : offset + rows], 0) for offset in range(kernel)]
    )
    scale = 1.0 / math.sqrt(total)
    stacked = (
        jnp.concatenate(
            [tap_terms, jnp.sum(grad_pre * normed, 0)[None], jnp.sum(grad_pre, 0)[None]], 0
        )
        * scale
    )
    summed = by_axis(stacked, SP)
    d_taps = summed[:kernel]
    d_gain = summed[kernel]
    d_shift = summed[kernel + 1]
    d_value = (grad_gated * gate_sig).astype(jnp.bfloat16)
    d_gate = (grad_gated * value_in.astype(jnp.float32) * gate_sig * (1.0 - gate_sig)).astype(
        jnp.bfloat16
    )
    return (d_value, d_gate, d_taps, d_gain, d_shift)


def solution(mesh):
    finer = Mesh(mesh.devices.reshape(12, 8, 4, mesh.shape["tp"]), ("sp_0", "sp_1", "sp_2", "tp"))
    return jax.shard_map(
        shards,
        mesh=finer,
        in_specs=(
            P(SP, "tp"),
            P(SP, "tp"),
            P(None, "tp"),
            P("tp"),
            P("tp"),
            P("tp", None),
            P(SP, None),
        ),
        out_specs=(P(SP, "tp"), P(SP, "tp"), P(None, "tp"), P("tp"), P("tp")),
        check_vma=False,
    )
```

profile of v0, /device:TPU:1, one launch (start us, length us, event | category | flops | bytes accessed | tf_op | source)
XLA Modules:
  0.0 335.4 jit_solution(16376318249576622349)
XLA Ops:
  7.2 0.0 copy-start.2
  7.2 0.0 copy-start.3
  7.2 0.0 all-reduce.5.cloned.1.call-start
  7.2 1.0 fusion.99
  8.2 3.9 %collective-permute-start = (bf16[30,1024]{1,0:T(8,128)(2,1)S(1)}, bf16[30,1024]{1,0:T(8,128)(2,1)S(1)}, u32[]{:S(2)}, u32[]{:S(2)}) collective-permute-start(bf16[30,1024]{1,0:T(8,128)(2,1)S(1)} %get-tuple-element.56), channel_id=1, source_target_pairs={{0,2},{2,4},{4,6},{6,8},{8,10},{10,12},{12,14},{14,16},{16,18},{18... | collective-permute-start | bytes 184328 | tf_op jit(solution)/shard_map/ppermute | solution.py:40
  12.1 1.3 collective-permute-start.1
  13.4 0.9 fusion.100
  14.3 4.0 %collective-permute-start.2 = (bf16[30,1024]{1,0:T(8,128)(2,1)S(1)}, bf16[30,1024]{1,0:T(8,128)(2,1)S(1)}, u32[]{:S(2)}, u32[]{:S(2)}) collective-permute-start(bf16[30,1024]{1,0:T(8,128)(2,1)S(1)} %get-tuple-element.58), channel_id=1, source_target_pairs={{0,2},{2,4},{4,6},{6,8},{8,10},{10,12},{12,14},{14,16},{16,18},{18... | collective-permute-start | bytes 184328 | tf_op jit(solution)/shard_map/ppermute | solution.py:40
  18.3 1.3 collective-permute-start.3
  19.6 1.7 fusion.98
  21.3 4.6 %collective-permute-start.4 = (bf16[30,2048]{1,0:T(8,128)(2,1)}, bf16[30,2048]{1,0:T(8,128)(2,1)}, u32[]{:S(2)}, u32[]{:S(2)}) collective-permute-start(bf16[30,2048]{1,0:T(8,128)(2,1)} %get-tuple-element.53), channel_id=1, source_target_pairs={{0,2},{2,4},{4,6},{6,8},{8,10},{10,12},{12,14},{14,16},{16,18},{18... | collective-permute-start | bytes 368648 | tf_op jit(solution)/shard_map/ppermute | solution.py:40
  26.0 1.3 fusion.102
  27.3 0.0 copy-start.5
  27.3 0.0 copy-start.6
  27.3 0.0 copy-start.7
  27.3 0.0 copy-start.8
  27.3 0.0 copy-start.9
  27.3 0.0 copy-start.10
  27.4 1.1 fusion.103
  28.6 0.0 copy-start.30
  28.7 0.0 copy-start.31
  28.7 0.0 collective-permute-done
  28.7 1.3 collective-permute-start.5
  30.0 0.0 collective-permute-done.1
  30.0 0.0 collective-permute-done.2
  30.0 0.0 collective-permute-done.3
  30.0 0.0 copy-done.2
  30.0 0.0 copy-done.3
  30.0 1.6 fusion.97
  31.8 5.7 %multiply_reduce_fusion.1 = (f32[286]{0:T(512)S(1)}, f32[286]{0:T(512)S(1)}, f32[286,1024]{1,0:T(8,128)S(1)}) fusion(f32[316,1024]{1,0:T(8,128)S(1)} %get-tuple-element.47, f32[1024]{0:T(1024)S(1)} %bitcast.125, f32[1024]{0:T(1024)S(1)} %bitcast.127, f32[1024]{0:T(1024)S(1)} %bitcast.69, f32[1024]{0:T(1024)S(1)} %bitcast.71, f32[1024]{0:T(1024)S(1)} %bitcast.73, ...), kind=kLoop, calls=%fused_computation.71 | loop fusion | flops 18742724 | bytes 37615856 | tf_op jit(solution)/shard_map/reduce_sum | solution.py:68
  37.6 11.1 %all-reduce = (f32[286]{0:T(512)S(1)}, f32[286]{0:T(512)S(1)}) all-reduce(f32[286]{0:T(512)S(1)} %get-tuple-element.41, f32[286]{0:T(512)S(1)} %get-tuple-element.40), channel_id=1, replica_groups=mesh['sp_0'=12,'sp_1'=8,'sp_2'=4,'tp'=2] {'tp'}, use_global_device_ids=true, to_apply=%region_3.0 | all-reduce | flops 572 | bytes 4576 | tf_op jit(solution)/shard_map/psum | solution.py:68
  48.7 0.2 subtract_multiply_fusion.1
  48.9 0.4 copy-done.32
  49.3 0.0 copy-done.33
  49.3 0.2 slice_convert_fusion
  49.4 0.0 collective-permute-done.4
  49.5 0.0 collective-permute-done.5
  49.5 1.0 copy-done.4
  50.5 4.2 %multiply_reduce_fusion.2 = (f32[286]{0:T(512)S(1)}, f32[286]{0:T(512)S(1)}, f32[286,1024]{1,0:T(8,128)S(1)}) fusion(f32[1024]{0:T(1024)S(1)} %copy-done.36, f32[286,1024]{1,0:T(8,128)S(1)} %subtract_multiply_fusion.1, f32[1024]{0:T(1024)S(1)} %copy-done.37, bf16[1024,2048]{1,0:T(8,128)(2,1)} %param.12, bf16[30,2048]{1,0:T(8,128)(2,1)} %collective-permute-done.5, ...), kind=kOutput, calls=%fused_computation.198 | convolution fusion | flops 1207184896 | bytes 7842032 | tf_op jit(solution)/shard_map/dot_general | solution.py:74
  54.7 1.0 slice_reduce_fusion
  55.7 0.0 copy-done.1
  55.8 0.1 pad_maximum_fusion.4
  55.8 3.7 %all_to_all.6 = f32[2,1,572]{2,1,0:T(1,128)S(1)} all-to-all(f32[2,1,572]{2,1,0:T(1,128)S(1)} %broadcast_in_dim.6), channel_id=1, replica_groups=mesh['sp_0'=12,'sp_1'=8,'sp_2'=4,'tp'=2] {'tp'}, dimensions={0} | all-to-all | bytes 9152 | tf_op jit(solution)/shard_map/all_to_all | solution.py:17
  59.5 0.1 slice_multiply_fusion.93
  59.6 1.7 subtract_multiply_fusion
  61.3 1.2 fusion.42
  62.5 1.2 fusion.51
  63.8 0.0 copy-start.34
  63.8 0.0 copy-start.35
  63.8 1.8 fusion.33
  65.7 0.3 concatenate.19
  65.9 0.7 broadcast_multiply_fusion
  66.6 0.0 all-reduce.5.cloned.1.call-update
  66.6 0.0 all-reduce.7.cloned.1.call-start
  66.7 112.7 %all-reduce.5.cloned.1.call-done = f32[33,1024]{1,0:T(8,128)} async-done(((f32[33,1024]{1,0:T(8,128)}), f32[33,1024]{1,0:T(8,128)}) %all-reduce.5.cloned.1.call-update) | async-done | bytes 135184 | tf_op jit(solution)/shard_map/psum | solution.py:50
  179.4 0.0 all-reduce.7.cloned.1.call-update
  179.4 0.2 all-reduce.9.cloned.1.call-start
  179.6 6.3 %multiply_convert_fusion.1 = (bf16[256,1024]{1,0:T(8,128)(2,1)}, f32[256,1024]{1,0:T(8,128)S(1)}) fusion(bf16[256,1024]{1,0:T(8,128)(2,1)} %param.7, f32[316,1024]{1,0:T(8,128)} %get-tuple-element.55, f32[286,1024]{1,0:T(8,128)S(1)} %subtract_multiply_fusion, f32[1024]{0:T(1024)} %bitcast.126, f32[1024]{0:T(1024)} %bitcast.128, f32[1024]{0:T(1024)S(1)} %bitcast.70, ...), kind=kLoop, calls=%fused_computation.196 | loop fusion | flops 17563648 | bytes 35778560 | tf_op jit(solution)/shard_map/convert_element_type | solution.py:129
  186.0 78.3 %all-reduce.7.cloned.1.call-done = f32[33,1024]{1,0:T(8,128)} async-done(((f32[33,1024]{1,0:T(8,128)}), f32[33,1024]{1,0:T(8,128)}) %all-reduce.7.cloned.1.call-update) | async-done | bytes 135184 | tf_op jit(solution)/shard_map/psum | solution.py:50
  264.2 0.0 all-reduce.9.cloned.1.call-update
  264.3 1.0 multiply_convert_fusion.2
  265.3 60.7 %all-reduce.9.cloned.1.call-done = f32[33,1024]{1,0:T(8,128)} async-done(((f32[33,1024]{1,0:T(8,128)}), f32[33,1024]{1,0:T(8,128)}) %all-reduce.9.cloned.1.call-update) | async-done | bytes 135184 | tf_op jit(solution)/shard_map/psum | solution.py:50
  326.0 1.6 slice.689
  327.5 1.4 fusion.101
  (61 shorter events, 0.2 us)
Async XLA Ops:
  7.2 22.8 %copy-start.2 = (bf16[256,1024]{1,0:T(8,128)(2,1)S(1)}, bf16[256,1024]{1,0:T(8,128)(2,1)}, u32[]{:S(2)}) copy-start(bf16[256,1024]{1,0:T(8,128)(2,1)} %param.7) | copy-start | bytes 1572868
  7.2 22.8 %copy-start.3 = (bf16[256,1024]{1,0:T(8,128)(2,1)S(1)}, bf16[256,1024]{1,0:T(8,128)(2,1)}, u32[]{:S(2)}) copy-start(bf16[256,1024]{1,0:T(8,128)(2,1)} %param.8) | copy-start | bytes 1572868
  7.2 172.2 %all-reduce.5.cloned.1.call-start = ((), (), s32[]{:S(2)}) async-start(), calls=%async_computation.1 | async-start | bytes 327680 | tf_op jit(solution)/shard_map/psum | solution.py:50
  8.2 20.5 %collective-permute-start = (bf16[30,1024]{1,0:T(8,128)(2,1)S(1)}, bf16[30,1024]{1,0:T(8,128)(2,1)S(1)}, u32[]{:S(2)}, u32[]{:S(2)}) collective-permute-start(bf16[30,1024]{1,0:T(8,128)(2,1)S(1)} %get-tuple-element.56), channel_id=1, source_target_pairs={{0,2},{2,4},{4,6},{6,8},{8,10},{10,12},{12,14},{14,16},{16,18},{18... | collective-permute-start | bytes 184328 | tf_op jit(solution)/shard_map/ppermute | solution.py:40
  12.1 17.8 %collective-permute-start.1 = (bf16[30,1024]{1,0:T(8,128)(2,1)S(1)}, bf16[30,1024]{1,0:T(8,128)(2,1)S(1)}, u32[]{:S(2)}, u32[]{:S(2)}) collective-permute-start(bf16[30,1024]{1,0:T(8,128)(2,1)S(1)} %get-tuple-element.57), channel_id=1, source_target_pairs={{2,0},{4,2},{6,4},{8,6},{10,8},{12,10},{14,12},{16,14},{18,16},{20... | collective-permute-start | bytes 184328 | tf_op jit(solution)/shard_map/ppermute | solution.py:43
  14.3 15.6 %collective-permute-start.2 = (bf16[30,1024]{1,0:T(8,128)(2,1)S(1)}, bf16[30,1024]{1,0:T(8,128)(2,1)S(1)}, u32[]{:S(2)}, u32[]{:S(2)}) collective-permute-start(bf16[30,1024]{1,0:T(8,128)(2,1)S(1)} %get-tuple-element.58), channel_id=1, source_target_pairs={{0,2},{2,4},{4,6},{6,8},{8,10},{10,12},{12,14},{14,16},{16,18},{18... | collective-permute-start | bytes 184328 | tf_op jit(solution)/shard_map/ppermute | solution.py:40
  18.3 11.7 %collective-permute-start.3 = (bf16[30,1024]{1,0:T(8,128)(2,1)S(1)}, bf16[30,1024]{1,0:T(8,128)(2,1)S(1)}, u32[]{:S(2)}, u32[]{:S(2)}) collective-permute-start(bf16[30,1024]{1,0:T(8,128)(2,1)S(1)} %get-tuple-element.59), channel_id=1, source_target_pairs={{2,0},{4,2},{6,4},{8,6},{10,8},{12,10},{14,12},{16,14},{18,16},{20... | collective-permute-start | bytes 184328 | tf_op jit(solution)/shard_map/ppermute | solution.py:43
  21.3 28.1 %collective-permute-start.4 = (bf16[30,2048]{1,0:T(8,128)(2,1)}, bf16[30,2048]{1,0:T(8,128)(2,1)}, u32[]{:S(2)}, u32[]{:S(2)}) collective-permute-start(bf16[30,2048]{1,0:T(8,128)(2,1)} %get-tuple-element.53), channel_id=1, source_target_pairs={{0,2},{2,4},{4,6},{6,8},{8,10},{10,12},{12,14},{14,16},{16,18},{18... | collective-permute-start | bytes 368648 | tf_op jit(solution)/shard_map/ppermute | solution.py:40
  27.3 4.3 %copy-start.5 = (f32[1,1024]{1,0:T(1,128)}, f32[1,1024]{1,0:T(1,128)S(1)}, u32[]{:S(2)}) copy-start(f32[1,1024]{1,0:T(1,128)S(1)} %get-tuple-element.66) | copy-start | bytes 12292
  27.3 4.3 %copy-start.6 = (f32[1,1024]{1,0:T(1,128)}, f32[1,1024]{1,0:T(1,128)S(1)}, u32[]{:S(2)}) copy-start(f32[1,1024]{1,0:T(1,128)S(1)} %get-tuple-element.67) | copy-start | bytes 12292
  27.3 4.3 %copy-start.7 = (f32[1,1024]{1,0:T(1,128)}, f32[1,1024]{1,0:T(1,128)S(1)}, u32[]{:S(2)}) copy-start(f32[1,1024]{1,0:T(1,128)S(1)} %get-tuple-element.68) | copy-start | bytes 12292
  27.3 4.3 %copy-start.8 = (f32[1,1024]{1,0:T(1,128)}, f32[1,1024]{1,0:T(1,128)S(1)}, u32[]{:S(2)}) copy-start(f32[1,1024]{1,0:T(1,128)S(1)} %get-tuple-element.69) | copy-start | bytes 12292
  27.3 4.3 %copy-start.9 = (f32[1,1024]{1,0:T(1,128)}, f32[1,1024]{1,0:T(1,128)S(1)}, u32[]{:S(2)}) copy-start(f32[1,1024]{1,0:T(1,128)S(1)} %get-tuple-element.70) | copy-start | bytes 12292
  27.3 4.3 %copy-start.10 = (f32[1,1024]{1,0:T(1,128)}, f32[1,1024]{1,0:T(1,128)S(1)}, u32[]{:S(2)}) copy-start(f32[1,1024]{1,0:T(1,128)S(1)} %get-tuple-element.71) | copy-start | bytes 12292
  27.4 4.3 %copy-start.11 = (f32[1,1024]{1,0:T(1,128)}, f32[1,1024]{1,0:T(1,128)S(1)}, u32[]{:S(2)}) copy-start(f32[1,1024]{1,0:T(1,128)S(1)} %get-tuple-element.72) | copy-start | bytes 12292
  27.4 4.3 %copy-start.12 = (f32[1,1024]{1,0:T(1,128)}, f32[1,1024]{1,0:T(1,128)S(1)}, u32[]{:S(2)}) copy-start(f32[1,1024]{1,0:T(1,128)S(1)} %get-tuple-element.73) | copy-start | bytes 12292
  27.4 4.3 %copy-start.13 = (f32[1,1024]{1,0:T(1,128)}, f32[1,1024]{1,0:T(1,128)S(1)}, u32[]{:S(2)}) copy-start(f32[1,1024]{1,0:T(1,128)S(1)} %get-tuple-element.74) | copy-start | bytes 12292
  27.4 4.3 %copy-start.14 = (f32[1,1024]{1,0:T(1,128)}, f32[1,1024]{1,0:T(1,128)S(1)}, u32[]{:S(2)}) copy-start(f32[1,1024]{1,0:T(1,128)S(1)} %get-tuple-element.75) | copy-start | bytes 12292
  27.4 4.3 %copy-start.15 = (f32[1,1024]{1,0:T(1,128)}, f32[1,1024]{1,0:T(1,128)S(1)}, u32[]{:S(2)}) copy-start(f32[1,1024]{1,0:T(1,128)S(1)} %get-tuple-element.76) | copy-start | bytes 12292
  27.4 4.3 %copy-start.16 = (f32[1,1024]{1,0:T(1,128)}, f32[1,1024]{1,0:T(1,128)S(1)}, u32[]{:S(2)}) copy-start(f32[1,1024]{1,0:T(1,128)S(1)} %get-tuple-element.77) | copy-start | bytes 12292
  27.4 4.3 %copy-start.17 = (f32[1,1024]{1,0:T(1,128)}, f32[1,1024]{1,0:T(1,128)S(1)}, u32[]{:S(2)}) copy-start(f32[1,1024]{1,0:T(1,128)S(1)} %get-tuple-element.78) | copy-start | bytes 12292
  27.4 4.3 %copy-start.18 = (f32[1,1024]{1,0:T(1,128)}, f32[1,1024]{1,0:T(1,128)S(1)}, u32[]{:S(2)}) copy-start(f32[1,1024]{1,0:T(1,128)S(1)} %get-tuple-element.79) | copy-start | bytes 12292
  27.4 4.3 %copy-start.19 = (f32[1,1024]{1,0:T(1,128)}, f32[1,1024]{1,0:T(1,128)S(1)}, u32[]{:S(2)}) copy-start(f32[1,1024]{1,0:T(1,128)S(1)} %get-tuple-element.80) | copy-start | bytes 12292
  28.5 3.2 copy-start.20
  28.5 3.2 copy-start.21
  28.6 3.2 copy-start.22
  28.6 3.2 copy-start.23
  28.6 3.2 copy-start.24
  28.6 3.2 copy-start.25
  28.6 3.2 copy-start.26
  28.6 3.2 copy-start.27
  28.6 3.2 copy-start.28
  28.6 3.2 copy-start.29
  28.6 3.2 copy-start.30
  28.7 3.2 copy-start.31
  28.7 20.8 %collective-permute-start.5 = (bf16[30,2048]{1,0:T(8,128)(2,1)}, bf16[30,2048]{1,0:T(8,128)(2,1)}, u32[]{:S(2)}, u32[]{:S(2)}) collective-permute-start(bf16[30,2048]{1,0:T(8,128)(2,1)} %get-tuple-element.54), channel_id=1, source_target_pairs={{2,0},{4,2},{6,4},{8,6},{10,8},{12,10},{14,12},{16,14},{18,16},{20... | collective-permute-start | bytes 368648 | tf_op jit(solution)/shard_map/ppermute | solution.py:43
  48.7 0.6 copy-start.32
  48.7 0.6 copy-start.33
  49.3 1.2 copy-start.4
  49.3 1.2 copy-start.36
  49.3 1.2 copy-start.37
  54.7 1.0 copy-start.1
  63.8 1.9 copy-start.34
  63.8 1.9 copy-start.35
  66.6 197.6 %all-reduce.7.cloned.1.call-start = ((), (), s32[]{:S(2)}) async-start(), calls=%async_computation.2 | async-start | bytes 327680 | tf_op jit(solution)/shard_map/psum | solution.py:50
  179.4 146.5 %all-reduce.9.cloned.1.call-start = ((), (), s32[]{:S(2)}) async-start(), calls=%async_computation.3 | async-start | bytes 327680 | tf_op jit(solution)/shard_map/psum | solution.py:50
  179.6 84.6 %copy-start = (f32[316,1024]{1,0:T(8,128)S(1)}, f32[316,1024]{1,0:T(8,128)}, u32[]{:S(2)}) copy-start(f32[316,1024]{1,0:T(8,128)} %get-tuple-element.55) | copy-start | bytes 3883012
Sparse Core Ops, SparseCore 0:
  66.7 112.5 all-reduce.4
  181.7 82.4 all-reduce.6
  266.6 59.3 all-reduce.8
where the time goes:
time: 337 us; the launch traced here: 335 us
  waiting for transfers between devices  252 us (75%)
  other arithmetic  22.8 us (7%)
  starting transfers between devices  16.7 us (5%)
  blocking collectives  14.8 us (4%)
  between operations  14.4 us (4%)
  local copies, waits for them, and re-layouts  10.8 us (3%)
  matrix products  4.22 us (1%)
    psum x3, waiting for transfers between devices, by_axis(): value = lax.psum(value, axis)  252 us
    ppermute x3, starting transfers between devices, with_halo(): lax.ppermute(lax.slice_in_dim(block, block.shape[dim] - width, None, axis...  12.6 us
    psum x1, blocking collectives, norm_backward(): lax.psum((jnp.sum(conv_out, 1), jnp.sum(conv_out * conv_out, 1)), 'tp')  11.1 us
  transfers between devices with their start and end apart: 9, of which 3 were waited for; matrix products, arithmetic and copies ran while one was open for 6% of the time, Pallas kernels for 0%

commit v1 on v0

v1 whole, which is shorter than its diff:
```python
import functools
import math

import jax
import jax.numpy as jnp
from jax import lax
from jax.experimental import pallas as pl
from jax.experimental.pallas import tpu as pltpu
from jax.sharding import Mesh
from jax.sharding import PartitionSpec as P

SP = ("sp_0", "sp_1", "sp_2")
EPS = 1e-05
F32 = jnp.float32
BF16 = jnp.bfloat16
MESH = pl.DeviceIdType.MESH

ROWS, WIDTH, KERNEL, HALF = 256, 1024, 31, 15
LANES, SUB, STEPS, PITCH, OUT_PITCH = 8, 8, 32, 72, 40
GROUP = 8


def position(dims):
    nz, ny, nx = dims
    z, y, x = (lax.axis_index(a) for a in SP)
    return z, y, x, lax.axis_index("tp"), (z * ny + y) * nx + x


def place(index, dims):
    nz, ny, nx = dims
    return {"sp_0": index // (ny * nx), "sp_1": (index // nx) % ny, "sp_2": index % nx}


def sigmoid(v):
    return jax.nn.sigmoid(v)


def kernel(
    dims,
    total,
    value_hbm, gate_hbm, taps_hbm, gain_hbm, shift_hbm, w_hbm, cot_hbm,
    d_value_hbm, d_gate_hbm, d_taps_hbm, d_gain_hbm, d_shift_hbm,
    value, gate, taps, gain, shift, w, cot,
    gated, conv, mix, grad, wide, back, parts, bits,
    edge_out, edge_in, tail_out, tail_in,
    stat_out, stat_in, mean_b, inv_b, first_b, second_b,
    tiles, tiles_in, line, final, shift_x, shift_y, shift_z, spare,
    d_value, d_gate, d_taps, d_gain, d_shift,
    in_sem, w_sem, edge_send, edge_recv, stat_send, stat_recv, tail_send, tail_recv,
    rs_send, rs_recv, z_send, z_recv, ag_send, ag_recv, sh_send, sh_recv, out_sem,
):
    nz, ny, nx = dims
    z, y, x, t, me = position(dims)
    n_sp = nz * ny * nx
    plane = ny * nx
    mine = x * ny + y
    after = place(lax.rem(me + 1, n_sp), dims)
    before = place(lax.rem(me + n_sp - 1, n_sp), dims)
    partner = {"tp": 1 - t}

    def in_plane(step):
        q = lax.rem(mine + step, plane)
        return q, {"sp_1": lax.rem(q, ny), "sp_2": q // ny}

    def along(axis, here, count, step):
        q = lax.rem(here + step, count)
        return q, {axis: q}

    barrier = pltpu.get_barrier_semaphore()

    def greet(device):
        pl.semaphore_signal(barrier, inc=1, device_id=device, device_id_type=MESH)

    greet(after)
    greet(before)
    greet(partner)

    @pl.loop(1, nz)
    def _(step):
        greet(along("sp_0", z, nz, step)[1])

    @pl.loop(1, plane)
    def _(step):
        greet(in_plane(step)[1])

    small = [
        pltpu.make_async_copy(src, dst, in_sem.at[i])
        for i, (src, dst) in enumerate(
            [(value_hbm, value), (gate_hbm, gate), (taps_hbm, taps), (gain_hbm, gain),
             (shift_hbm, shift), (cot_hbm, cot)]
        )
    ]
    big = [
        pltpu.make_async_copy(
            w_hbm.at[pl.ds(256 * i, 256)], w.at[pl.ds(256 * i, 256)], w_sem.at[i]
        )
        for i in range(4)
    ]
    small[0].start()
    small[1].start()
    small[5].start()
    for copy in big:
        copy.start()
    for i in (2, 3, 4):
        small[i].start()

    small[0].wait()
    small[1].wait()

    def gated_of(rows, lanes):
        sig = sigmoid(gate[rows, lanes].astype(F32))
        return (value[rows, lanes].astype(F32) * sig).astype(BF16)

    for i, start in enumerate((0, ROWS - 16)):
        edge_out[i] = gated_of(pl.ds(start, 16), slice(None))

    @pl.loop(0, SUB)
    def _(s):
        for half in range(2):
            rows = pl.ds(pl.multiple_of(32 * s + 16 * half, 16), 16)
            for l in range(LANES):
                v = gated_of(rows, slice(128 * l, 128 * l + 128)).astype(F32)
                own = pl.multiple_of(PITCH * (s + 1) + 16 + 16 * half, 8)
                gated[l, pl.ds(own, 16)] = v
                other = pl.multiple_of(PITCH * s + 48 if half == 0 else PITCH * (s + 2), 8)
                gated[l, pl.ds(other, 16)] = v

    small[5].wait()
    for i in range(4):
        big[i].wait()
        for part in range(2):
            l = 2 * i + part
            product = lax.dot_general(
                cot[...], w[pl.ds(128 * l, 128)], (((1,), (1,)), ((), ())),
                preferred_element_type=F32,
            )
            for s in range(SUB):
                mix[l, pl.ds(OUT_PITCH * s, 32)] = product[32 * s : 32 * s + 32]

    for i in (2, 3, 4):
        small[i].wait()

    pl.semaphore_wait(barrier, (nz - 1) + (plane - 1) + 3)

    def exchange(source, target, send, recv, device):
        return pltpu.make_async_remote_copy(
            src_ref=source, dst_ref=target, send_sem=send, recv_sem=recv,
            device_id=device, device_id_type=MESH,
        )

    edges = [
        exchange(edge_out.at[0], edge_in.at[1], edge_send.at[0], edge_recv.at[1], before),
        exchange(edge_out.at[1], edge_in.at[0], edge_send.at[1], edge_recv.at[0], after),
    ]
    for copy in edges:
        copy.start()
    for copy in edges:
        copy.wait()
    absent = (me == 0, me == n_sp - 1)
    for i, start in enumerate((PITCH, SUB * PITCH + 48)):
        for l in range(LANES):
            v = edge_in[i, :, 128 * l : 128 * l + 128].astype(F32)
            gated[l, pl.ds(start, 16)] = jnp.where(absent[i], 0.0, v)

    def tap(k, l):
        lanes = pl.ds(pl.multiple_of(128 * l, 128), 128)
        return jnp.broadcast_to(taps[pl.ds(k, 1), lanes], (SUB, 128))

    @pl.loop(0, LANES)
    def _(l):
        for j0 in range(0, STEPS, GROUP):
            window = [
                gated[l, pl.ds(PITCH + j0 + 1 + i, SUB, stride=PITCH)]
                for i in range(GROUP + KERNEL - 1)
            ]
            sums = [jnp.zeros((SUB, 128), F32)] * GROUP
            for k in range(KERNEL):
                weight = tap(k, l)
                for i in range(GROUP):
                    sums[i] = sums[i] + weight * window[i + k]
            for i in range(GROUP):
                conv[l, pl.ds(8 * (j0 + i), 8)] = sums[i]

    lane = lax.broadcasted_iota(jnp.int32, (SUB, 128), 1)
    zero = jnp.zeros((SUB, 128), F32)

    def at_row(j):
        return pl.ds(pl.multiple_of(8 * j, 8), 8)

    def put(packed, j, v):
        return jnp.where(lane == j, jnp.sum(v, 1, keepdims=True), packed)

    def of_pair(slot):
        copy = exchange(
            stat_out.at[slot], stat_in.at[slot], stat_send.at[slot], stat_recv.at[slot], partner
        )
        copy.start()
        copy.wait()
        return (
            stat_out[slot, 0] + stat_in[slot, 0],
            stat_out[slot, 1] + stat_in[slot, 1],
        )

    def spread(packed, target):
        for j in range(STEPS):
            target[8 * j : 8 * j + 8] = jnp.broadcast_to(packed[:, j : j + 1], (SUB, 128))

    def totals(j, carry):
        one, two = zero, zero
        for l in range(LANES):
            v = conv[l, at_row(j)]
            one = one + v
            two = two + v * v
        return put(carry[0], j, one), put(carry[1], j, two)

    one, two = lax.fori_loop(0, STEPS, totals, (zero, zero))
    stat_out[0, 0] = one
    stat_out[0, 1] = two
    one, two = of_pair(0)
    width = 2.0 * WIDTH
    mean = one / width
    inv = lax.rsqrt(two / width - mean * mean + EPS)
    spread(mean, mean_b)
    spread(inv, inv_b)

    def norm(j, carry):
        packed_one, packed_two, by_gain, by_shift = carry
        by_gain, by_shift = list(by_gain), list(by_shift)
        mean, inv = mean_b[at_row(j)], inv_b[at_row(j)]
        one, two = zero, zero
        for l in range(LANES):
            lanes = slice(128 * l, 128 * l + 128)
            g = gain[:, lanes]
            normed = (conv[l, at_row(j)] - mean) * inv
            pre = normed * g + shift[:, lanes]
            sig = sigmoid(pre)
            grad_pre = mix[l, pl.ds(j, SUB, stride=OUT_PITCH)] * sig * (1.0 + pre * (1.0 - sig))
            grad_normed = grad_pre * g
            one = one + grad_normed
            two = two + grad_normed * normed
            by_gain[l] = by_gain[l] + grad_pre * normed
            by_shift[l] = by_shift[l] + grad_pre
            conv[l, at_row(j)] = normed
            grad[l, at_row(j)] = grad_normed
        return (
            put(packed_one, j, one), put(packed_two, j, two), tuple(by_gain), tuple(by_shift)
        )

    one, two, by_gain, by_shift = lax.fori_loop(
        0, STEPS, norm, (zero, zero, (zero,) * LANES, (zero,) * LANES)
    )
    stat_out[1, 0] = one
    stat_out[1, 1] = two
    for l in range(LANES):
        parts[l, 8 * KERNEL : 8 * KERNEL + 8] = by_gain[l]
        spare[8 * l : 8 * l + 8] = by_shift[l]
    one, two = of_pair(1)
    spread(one / width, first_b)
    spread(two / width, second_b)

    def folded(ref, start):
        rows = ref[pl.ds(start, 8, stride=8)]
        for s in range(1, SUB):
            rows = rows + ref[pl.ds(start + s, 8, stride=8)]
        return rows

    def to_axis(buffer, axis, here, count, index):
        def descriptor(step):
            _, device = along(axis, here, count, step)
            return exchange(
                buffer.at[here], buffer.at[here], sh_send.at[index], sh_recv.at[index], device
            )

        @pl.loop(1, count)
        def _(step):
            descriptor(step).start()

    def arrived(buffer, count, send, recv):
        if count > 1:
            some = buffer.at[pl.ds(0, count - 1)]
            pltpu.make_async_copy(some, some, recv).wait()
            pltpu.make_async_copy(some, some, send).wait()

    def from_axis(buffer, count, index):
        arrived(buffer, count, sh_send.at[index], sh_recv.at[index])
        result = buffer[0]
        for i in range(1, count):
            result = result + buffer[i]
        return result

    shift_x[x] = folded(spare, 0)
    to_axis(shift_x, "sp_2", x, nx, 0)

    @pl.loop(0, STEPS)
    def _(j):
        inv, one, two = inv_b[at_row(j)], first_b[at_row(j)], second_b[at_row(j)]
        for l in range(LANES):
            v = inv * (grad[l, at_row(j)] - one - conv[l, at_row(j)] * two)
            grad[l, at_row(j)] = v
            wide[l, pl.ds(PITCH + 16 + j, SUB, stride=PITCH)] = v
            wide[l, pl.ds(j + 48 + 80 * (j // 16), SUB, stride=PITCH)] = v

    for l in range(LANES):
        tail_out[0, l] = wide[l, 48:64]
        tail_out[1, l] = wide[l, 9 * PITCH : 9 * PITCH + 16]

    shift_y[y] = from_axis(shift_x, nx, 0)
    to_axis(shift_y, "sp_1", y, ny, 1)
    tails = [
        exchange(tail_out.at[0], tail_in.at[1], tail_send.at[0], tail_recv.at[1], before),
        exchange(tail_out.at[1], tail_in.at[0], tail_send.at[1], tail_recv.at[0], after),
    ]
    for copy in tails:
        copy.start()

    @pl.loop(0, LANES)
    def _(l):
        for k0 in range(0, KERNEL, GROUP):
            count = min(GROUP, KERNEL - k0)
            sums = [zero] * count
            window = [
                gated[l, pl.ds(PITCH + 1 + k0 + i, SUB, stride=PITCH)]
                for i in range(STEPS + count - 1)
            ]
            for j in range(STEPS):
                g = grad[l, pl.ds(8 * j, 8)]
                for i in range(count):
                    sums[i] = sums[i] + g * window[j + i]
            for i in range(count):
                parts[l, pl.ds(8 * (k0 + i), 8)] = sums[i]
        for g in range(4):
            tiles[g * LANES + l] = folded(parts.at[l], 64 * g)

    shift_z[z] = from_axis(shift_y, ny, 1)

    @pl.loop(1, plane)
    def _(step):
        q, device = in_plane(step)
        exchange(tiles.at[q], tiles_in.at[mine], rs_send, rs_recv, device).start()

    to_axis(shift_z, "sp_0", z, nz, 2)

    for copy in tails:
        copy.wait()
    for i, start in enumerate((PITCH, SUB * PITCH + 48)):
        for l in range(LANES):
            wide[l, pl.ds(start, 16)] = jnp.where(absent[i], 0.0, tail_in[i, l])

    @pl.loop(0, LANES)
    def _(l):
        for j0 in range(0, STEPS, GROUP):
            low = PITCH + 31 - (KERNEL - 1) + j0
            window = [
                wide[l, pl.ds(low + i, SUB, stride=PITCH)] for i in range(GROUP + KERNEL - 1)
            ]
            sums = [zero] * GROUP
            for k in range(KERNEL):
                weight = tap(k, l)
                for i in range(GROUP):
                    sums[i] = sums[i] + weight * window[i + KERNEL - 1 - k]
            for i in range(GROUP):
                back[l, pl.ds(j0 + i, SUB, stride=OUT_PITCH)] = sums[i]

    @pl.loop(0, SUB)
    def _(s):
        for half in range(2):
            rows = pl.ds(pl.multiple_of(32 * s + 16 * half, 16), 16)
            for l in range(LANES):
                lanes = slice(128 * l, 128 * l + 128)
                g = back[l, pl.ds(pl.multiple_of(OUT_PITCH * s + 16 * half, 8), 16)]
                sig = sigmoid(gate[rows, lanes].astype(F32))
                d_value[rows, lanes] = (g * sig).astype(BF16)
                d_gate[rows, lanes] = (
                    g * value[rows, lanes].astype(F32) * sig * (1.0 - sig)
                ).astype(BF16)

    outs = [
        pltpu.make_async_copy(src, dst, out_sem.at[i])
        for i, (src, dst) in enumerate(
            [(d_value, d_value_hbm), (d_gate, d_gate_hbm), (d_taps, d_taps_hbm),
             (d_gain, d_gain_hbm), (d_shift, d_shift_hbm)]
        )
    ]
    outs[0].start()
    outs[1].start()

    scale = 1.0 / math.sqrt(total)
    arrived(tiles_in, plane, rs_send, rs_recv)
    line_own = tiles[mine]
    tiles_in[mine] = line_own
    halves = [tiles_in[0], tiles_in[1]]
    for i in range(2, plane):
        halves[i % 2] = halves[i % 2] + tiles_in[i]
    line[z] = halves[0] + halves[1]

    @pl.loop(1, nz)
    def _(step):
        _, device = along("sp_0", z, nz, step)
        exchange(line.at[z], line.at[z], z_send, z_recv, device).start()

    d_shift[...] = from_axis(shift_z, nz, 2) * scale
    outs[4].start()

    arrived(line, nz, z_send, z_recv)
    result = line[0]
    for i in range(1, nz):
        result = result + line[i]
    final[mine] = result * scale

    @pl.loop(1, plane)
    def _(step):
        _, device = in_plane(step)
        exchange(final.at[mine], final.at[mine], ag_send, ag_recv, device).start()

    arrived(final, plane, ag_send, ag_recv)
    for g in range(4):
        for l in range(LANES):
            lanes = slice(128 * l, 128 * l + 128)
            if g < 3:
                d_taps[8 * g : 8 * g + 8, lanes] = final[g * LANES + l]
            else:
                last = final[g * LANES + l]
                d_taps[24:KERNEL, lanes] = last[:7]
                d_gain[:, lanes] = last[7:]
    outs[2].start()
    outs[3].start()
    for copy in outs:
        copy.wait()


def shards(dims, total, value_in, gate_in, taps, gain, shift, w_out, grad_out):
    nz, ny, nx = dims
    depth = grad_out.shape[1]
    vmem = pltpu.VMEM
    dma = pltpu.SemaphoreType.DMA
    padded = (LANES, 10 * PITCH, 128)
    rows = (LANES, ROWS, 128)
    spread = (LANES, SUB * OUT_PITCH, 128)
    scratch = [
        vmem((ROWS, WIDTH), BF16), vmem((ROWS, WIDTH), BF16), vmem((KERNEL, WIDTH), F32),
        vmem((1, WIDTH), F32), vmem((1, WIDTH), F32), vmem((WIDTH, depth), BF16),
        vmem((ROWS, depth), BF16),
        vmem(padded, F32), vmem(rows, F32), vmem(spread, F32), vmem(rows, F32),
        vmem(padded, F32), vmem(spread, F32), vmem(rows, F32), vmem((8, 128), F32),
        vmem((2, 16, WIDTH), BF16), vmem((2, 16, WIDTH), BF16),
        vmem((2, LANES, 16, 128), F32), vmem((2, LANES, 16, 128), F32),
        vmem((2, 2, SUB, 128), F32), vmem((2, 2, SUB, 128), F32),
        vmem((ROWS, 128), F32), vmem((ROWS, 128), F32), vmem((ROWS, 128), F32),
        vmem((ROWS, 128), F32),
        vmem((32, 8, 128), F32), vmem((32, 8, 128), F32), vmem((nz, 8, 128), F32),
        vmem((32, 8, 128), F32), vmem((nx, 8, 128), F32), vmem((ny, 8, 128), F32),
        vmem((nz, 8, 128), F32), vmem((64, 128), F32),
        vmem((ROWS, WIDTH), BF16), vmem((ROWS, WIDTH), BF16), vmem((KERNEL, WIDTH), F32),
        vmem((1, WIDTH), F32), vmem((8, 128), F32),
        dma((6,)), dma((4,)), dma((2,)), dma((2,)), dma((2,)), dma((2,)), dma((2,)), dma((2,)),
        dma, dma, dma, dma, dma, dma, dma((3,)), dma((3,)), dma((5,)),
    ]
    anywhere = pl.BlockSpec(memory_space=pl.ANY)
    shape = jax.ShapeDtypeStruct
    d_value, d_gate, d_taps, d_gain, d_shift = pl.pallas_call(
        functools.partial(kernel, dims, total),
        out_shape=(
            shape((ROWS, WIDTH), BF16), shape((ROWS, WIDTH), BF16), shape((KERNEL, WIDTH), F32),
            shape((1, WIDTH), F32), shape((8, 128), F32),
        ),
        in_specs=[anywhere] * 7,
        out_specs=(anywhere,) * 5,
        scratch_shapes=scratch,
        compiler_params=pltpu.CompilerParams(
            collective_id=0, has_side_effects=True, vmem_limit_bytes=48 * 2**20
        ),
        name="module",
    )(value_in, gate_in, taps, gain.reshape(1, WIDTH), shift.reshape(1, WIDTH), w_out, grad_out)
    return d_value, d_gate, d_taps, d_gain.reshape(WIDTH), d_shift.reshape(WIDTH)


def solution(mesh, dims=(12, 8, 4)):
    finer = Mesh(mesh.devices.reshape(*dims, mesh.shape["tp"]), (*SP, "tp"))
    total = ROWS * math.prod(dims)
    return jax.shard_map(
        functools.partial(shards, dims, total),
        mesh=finer,
        in_specs=(
            P(SP, "tp"), P(SP, "tp"), P(None, "tp"), P("tp"), P("tp"), P("tp", None), P(SP, None),
        ),
        out_specs=(P(SP, "tp"), P(SP, "tp"), P(None, "tp"), P("tp"), P("tp")),
        check_vma=False,
    )
```

time: 337 us -> 72.3 us (0.21)
  the two profiles are of different devices: /device:TPU:1 before, /device:TPU:8 now
where the time goes in v1:
time: 72.3 us; the launch traced here: 71.9 us
  Pallas kernels  62.3 us (86%)
  local copies, waits for them, and re-layouts  9.01 us (12%)
    pallas_call x1, Pallas kernels, shards(): pl.pallas_call(functools.partial(kernel, dims, total), out_shape=(shape((...  62.3 us
    unnamed x17, local copies, waits for them, and re-layouts  9.01 us

profile of v1, /device:TPU:8, one launch (start us, length us, event | category | flops | bytes accessed | tf_op | source)
XLA Modules:
  0.0 71.9 jit_solution(6749663946893464312)
XLA Ops:
  0.6 0.0 copy-start
  0.6 1.2 %copy-done = bf16[256,2048]{1,0:T(8,128)(2,1)S(1)} copy-done((bf16[256,2048]{1,0:T(8,128)(2,1)S(1)}, bf16[256,2048]{1,0:T(8,128)(2,1)}, u32[]{:S(2)}) %copy-start) | copy-done | bytes 1048600
  1.9 0.0 copy-start.1
  1.9 1.0 %copy-done.1 = bf16[256,1024]{1,0:T(8,128)(2,1)S(1)} copy-done((bf16[256,1024]{1,0:T(8,128)(2,1)S(1)}, bf16[256,1024]{1,0:T(8,128)(2,1)}, u32[]{:S(2)}) %copy-start.1) | copy-done | bytes 524312
  2.9 0.0 copy-start.2
  2.9 1.0 %copy-done.2 = bf16[256,1024]{1,0:T(8,128)(2,1)S(1)} copy-done((bf16[256,1024]{1,0:T(8,128)(2,1)S(1)}, bf16[256,1024]{1,0:T(8,128)(2,1)}, u32[]{:S(2)}) %copy-start.2) | copy-done | bytes 524312
  3.9 0.0 copy-start.3
  3.9 0.9 %copy-done.3 = f32[31,1024]{1,0:T(8,128)S(1)} copy-done((f32[31,1024]{1,0:T(8,128)S(1)}, f32[31,1024]{1,0:T(8,128)}, u32[]{:S(2)}) %copy-start.3) | copy-done | bytes 127000
  4.8 0.0 copy-start.4
  4.9 0.7 copy-done.4
  5.5 0.0 copy-start.5
  5.5 0.7 copy-done.5
  6.2 62.3 %module.1 = (bf16[256,1024]{1,0:T(8,128)(2,1)S(1)}, bf16[256,1024]{1,0:T(8,128)(2,1)S(1)}, f32[31,1024]{1,0:T(8,128)S(1)}, f32[1,1024]{1,0:T(1,128)S(1)}, f32[8,128]{1,0:T(8,128)S(1)}) custom-call(bf16[256,1024]{1,0:T(8,128)(2,1)S(1)} %copy-done.1, bf16[256,1024]{1,0:T(8,128)(2,1)S(1)} %copy-done.2, f32[31,1024]{1,0:T(8,128)S(1)} %copy-done.3, ...), custom_call_target="tpu_custom_call" | custom-call | tf_op jit(solution)/shard_map/module/pallas_call | solution.py:460
  68.5 0.8 %copy.17 = bf16[256,1024]{1,0:T(8,128)(2,1)} copy(bf16[256,1024]{1,0:T(8,128)(2,1)S(1)} %get-tuple-element.20) | data formatting | bytes 1048576
  69.3 0.8 %copy.18 = bf16[256,1024]{1,0:T(8,128)(2,1)} copy(bf16[256,1024]{1,0:T(8,128)(2,1)S(1)} %get-tuple-element.21) | data formatting | bytes 1048576
  70.1 0.7 copy.19
  70.7 0.6 copy.20
  71.3 0.6 copy.21
Async XLA Ops:
  0.6 1.2 %copy-start = (bf16[256,2048]{1,0:T(8,128)(2,1)S(1)}, bf16[256,2048]{1,0:T(8,128)(2,1)}, u32[]{:S(2)}) copy-start(bf16[256,2048]{1,0:T(8,128)(2,1)} %cot_hbm.1) | copy-start | bytes 3145732
  1.9 1.0 %copy-start.1 = (bf16[256,1024]{1,0:T(8,128)(2,1)S(1)}, bf16[256,1024]{1,0:T(8,128)(2,1)}, u32[]{:S(2)}) copy-start(bf16[256,1024]{1,0:T(8,128)(2,1)} %value_hbm.1) | copy-start | bytes 1572868
  2.9 1.0 %copy-start.2 = (bf16[256,1024]{1,0:T(8,128)(2,1)S(1)}, bf16[256,1024]{1,0:T(8,128)(2,1)}, u32[]{:S(2)}) copy-start(bf16[256,1024]{1,0:T(8,128)(2,1)} %gate_hbm.1) | copy-start | bytes 1572868
  3.9 0.9 %copy-start.3 = (f32[31,1024]{1,0:T(8,128)S(1)}, f32[31,1024]{1,0:T(8,128)}, u32[]{:S(2)}) copy-start(f32[31,1024]{1,0:T(8,128)} %taps_hbm.1) | copy-start | bytes 380932
  4.8 0.7 copy-start.4
  5.5 0.7 copy-start.5

commit v2 on v1

v2 whole, which is shorter than its diff:
```python
import functools
import math

import jax
import jax.numpy as jnp
from jax import lax
from jax.experimental import pallas as pl
from jax.experimental.pallas import tpu as pltpu
from jax.sharding import Mesh
from jax.sharding import PartitionSpec as P

SP = ("sp_0", "sp_1", "sp_2")
EPS = 1e-05
F32 = jnp.float32
BF16 = jnp.bfloat16
MESH = pl.DeviceIdType.MESH

ROWS, WIDTH, KERNEL, HALF = 256, 1024, 31, 15
LANES, SUB, STEPS, PITCH, OUT_PITCH = 8, 8, 32, 72, 40
GROUP = 8


def position(dims):
    nz, ny, nx = dims
    z, y, x = (lax.axis_index(a) for a in SP)
    return z, y, x, lax.axis_index("tp"), (z * ny + y) * nx + x


def place(index, dims):
    nz, ny, nx = dims
    return {"sp_0": index // (ny * nx), "sp_1": (index // nx) % ny, "sp_2": index % nx}


def sigmoid(v):
    return jax.nn.sigmoid(v)


class Phases:
    def __init__(self):
        self.open = None

    def __call__(self, name):
        if self.open is not None:
            self.open.__exit__(None, None, None)
        self.open = None if name is None else jax.named_scope(name)
        if self.open is not None:
            self.open.__enter__()


def kernel(
    dims,
    total,
    value_hbm, gate_hbm, taps_hbm, gain_hbm, shift_hbm, w_hbm, cot_hbm,
    d_value, d_gate, d_taps, d_gain, d_shift,
    value, gate, taps, gain, shift, w, cot,
    gated, conv, mix, grad, wide, back, parts, bits,
    edge_out, edge_in, edge, tail_out, tail_in,
    stat_out, stat_in, mean_b, inv_b, first_b, second_b,
    tiles, tiles_in, line, final, shift_x, shift_y, shift_z, spare,
    in_sem, w_sem, edge_send, edge_recv, stat_send, stat_recv, tail_send, tail_recv,
    rs_send, rs_recv, z_send, z_recv, ag_send, ag_recv, sh_send, sh_recv,
):
    nz, ny, nx = dims
    z, y, x, t, me = position(dims)
    n_sp = nz * ny * nx
    plane = ny * nx
    mine = x * ny + y
    after = place(lax.rem(me + 1, n_sp), dims)
    before = place(lax.rem(me + n_sp - 1, n_sp), dims)
    partner = {"tp": 1 - t}

    def far_first(count):
        return sorted(range(1, count), key=lambda step: -min(step, count - step))

    def ring(here, count):
        return [here] + [lax.rem(here + step, count) for step in range(1, count)]

    xs, ys, zs = ring(x, nx), ring(y, ny), ring(z, nz)
    in_plane = [
        {"sp_1": ys[dy], "sp_2": xs[dx]}
        for dx, dy in sorted(
            [(dx, dy) for dx in range(nx) for dy in range(ny) if dx or dy],
            key=lambda d: -(min(d[0], nx - d[0]) + min(d[1], ny - d[1])),
        )
    ]

    def along(axis, places):
        return [{axis: places[step]} for step in far_first(len(places))]

    phase = Phases()

    small = [
        pltpu.make_async_copy(src, dst, in_sem.at[i])
        for i, (src, dst) in enumerate(
            [(value_hbm, value), (gate_hbm, gate), (taps_hbm, taps), (gain_hbm, gain),
             (shift_hbm, shift), (cot_hbm, cot)]
        )
    ]
    big = [
        pltpu.make_async_copy(
            w_hbm.at[pl.ds(256 * i, 256)], w.at[pl.ds(256 * i, 256)], w_sem.at[i]
        )
        for i in range(4)
    ]
    small[0].start()
    small[1].start()
    small[5].start()
    for copy in big:
        copy.start()
    for i in (2, 3, 4):
        small[i].start()

    phase("greet")
    barrier = pltpu.get_barrier_semaphore()

    def greet(device):
        pl.semaphore_signal(barrier, inc=1, device_id=device, device_id_type=MESH)

    for device in along("sp_0", zs) + in_plane + [after, before, partner]:
        greet(device)

    phase("load")
    small[0].wait()
    small[1].wait()

    def gated_of(rows, lanes):
        sig = sigmoid(gate[rows, lanes].astype(F32))
        return (value[rows, lanes].astype(F32) * sig).astype(BF16)

    phase("gate")
    for i, start in enumerate((0, ROWS - 16)):
        edge_out[i] = gated_of(pl.ds(start, 16), slice(None))

    starts = (PITCH, SUB * PITCH + 48)
    for l in range(LANES):
        for start in starts:
            gated[l, pl.ds(start, 16)] = jnp.zeros((16, 128), F32)
        edge[l, 16:32] = jnp.zeros((16, 128), F32)

    @pl.loop(0, SUB)
    def _(s):
        for half in range(2):
            rows = pl.ds(pl.multiple_of(32 * s + 16 * half, 16), 16)
            for l in range(LANES):
                v = gated_of(rows, slice(128 * l, 128 * l + 128)).astype(F32)
                own = pl.multiple_of(PITCH * (s + 1) + 16 + 16 * half, 8)
                gated[l, pl.ds(own, 16)] = v
                other = pl.multiple_of(PITCH * s + 48 if half == 0 else PITCH * (s + 2), 8)
                gated[l, pl.ds(other, 16)] = v

    phase("project")
    small[5].wait()
    for i in range(4):
        big[i].wait()
        product = lax.dot_general(
            cot[...], w[pl.ds(256 * i, 256)], (((1,), (1,)), ((), ())),
            preferred_element_type=F32,
        )
        for part in range(2):
            for s in range(SUB):
                mix[2 * i + part, pl.ds(OUT_PITCH * s, 32)] = product[
                    32 * s : 32 * s + 32, 128 * part : 128 * part + 128
                ]

    for i in (2, 3, 4):
        small[i].wait()

    phase("barrier")
    pl.semaphore_wait(barrier, (nz - 1) + (plane - 1) + 3)

    def exchange(source, target, send, recv, device):
        return pltpu.make_async_remote_copy(
            src_ref=source, dst_ref=target, send_sem=send, recv_sem=recv,
            device_id=device, device_id_type=MESH,
        )

    phase("edges")
    edges = [
        exchange(edge_out.at[0], edge_in.at[1], edge_send.at[0], edge_recv.at[1], before),
        exchange(edge_out.at[1], edge_in.at[0], edge_send.at[1], edge_recv.at[0], after),
    ]
    for copy in edges:
        copy.start()
    def tap(k, l):
        lanes = pl.ds(pl.multiple_of(128 * l, 128), 128)
        return jnp.broadcast_to(taps[pl.ds(k, 1), lanes], (SUB, 128))

    phase("conv")
    @pl.loop(0, LANES)
    def _(l):
        for j0 in range(0, STEPS, GROUP):
            window = [
                gated[l, pl.ds(PITCH + j0 + 1 + i, SUB, stride=PITCH)]
                for i in range(GROUP + KERNEL - 1)
            ]
            sums = [jnp.zeros((SUB, 128), F32)] * GROUP
            for k in range(KERNEL):
                weight = tap(k, l)
                for i in range(GROUP):
                    sums[i] = sums[i] + weight * window[i + k]
            for i in range(GROUP):
                conv[l, pl.ds(8 * (j0 + i), 8)] = sums[i]

    phase("edges_wait")
    for copy in edges:
        copy.wait()
    phase("fill")
    absent = (me == 0, me == n_sp - 1)
    for i in range(2):
        for l in range(LANES):
            v = edge_in[i, :, 128 * l : 128 * l + 128].astype(F32)
            v = jnp.where(absent[i], 0.0, v)
            gated[l, pl.ds(starts[i], 16)] = v
            edge[l, pl.ds(32 * i, 16)] = v

    @pl.loop(0, LANES)
    def _(l):
        for t0 in (0, 8):
            low = jnp.zeros((SUB, 128), F32)
            for k in range(HALF - t0):
                low = low + tap(k, l) * edge[l, pl.ds(t0 + k + 1, 8)]
            rows = pl.ds(8 * t0, 8, stride=8)
            conv[l, rows] = conv[l, rows] + low
            high = jnp.zeros((SUB, 128), F32)
            for k in range(24 - t0, KERNEL):
                high = high + tap(k, l) * edge[l, pl.ds(t0 + k + 1, 8)]
            rows = pl.ds(8 * (16 + t0) + 7, 8, stride=8)
            conv[l, rows] = conv[l, rows] + high

    lane = lax.broadcasted_iota(jnp.int32, (SUB, 128), 1)
    zero = jnp.zeros((SUB, 128), F32)

    def at_row(j):
        return pl.ds(pl.multiple_of(8 * j, 8), 8)

    def packed(ref):
        result = zero
        for j in range(STEPS):
            row = jnp.sum(ref[8 * j : 8 * j + 8], 1, keepdims=True)
            result = jnp.where(lane == j, row, result)
        return result

    def of_pair(slot):
        copy = exchange(
            stat_out.at[slot], stat_in.at[slot], stat_send.at[slot], stat_recv.at[slot], partner
        )
        copy.start()
        copy.wait()
        return (
            stat_out[slot, 0] + stat_in[slot, 0],
            stat_out[slot, 1] + stat_in[slot, 1],
        )

    def spread(stat, target):
        for j in range(STEPS):
            target[8 * j : 8 * j + 8] = jnp.broadcast_to(stat[:, j : j + 1], (SUB, 128))

    phase("totals")

    @pl.loop(0, STEPS, unroll=4)
    def _(j):
        one, two = zero, zero
        for l in range(LANES):
            v = conv[l, at_row(j)]
            one = one + v
            two = two + v * v
        first_b[at_row(j)] = one
        second_b[at_row(j)] = two

    stat_out[0, 0] = packed(first_b)
    stat_out[0, 1] = packed(second_b)
    phase("pair0")
    one, two = of_pair(0)
    phase("spread0")
    width = 2.0 * WIDTH
    mean = one / width
    inv = lax.rsqrt(two / width - mean * mean + EPS)
    spread(mean, mean_b)
    spread(inv, inv_b)

    def norm(j, carry):
        by_gain, by_shift = (list(part) for part in carry)
        mean, inv = mean_b[at_row(j)], inv_b[at_row(j)]
        one, two = zero, zero
        for l in range(LANES):
            lanes = slice(128 * l, 128 * l + 128)
            g = gain[:, lanes]
            normed = (conv[l, at_row(j)] - mean) * inv
            pre = normed * g + shift[:, lanes]
            sig = sigmoid(pre)
            grad_pre = mix[l, pl.ds(j, SUB, stride=OUT_PITCH)] * sig * (1.0 + pre * (1.0 - sig))
            grad_normed = grad_pre * g
            one = one + grad_normed
            two = two + grad_normed * normed
            by_gain[l] = by_gain[l] + grad_pre * normed
            by_shift[l] = by_shift[l] + grad_pre
            conv[l, at_row(j)] = normed
            grad[l, at_row(j)] = grad_normed
        first_b[at_row(j)] = one
        second_b[at_row(j)] = two
        return tuple(by_gain), tuple(by_shift)

    phase("norm")
    by_gain, by_shift = lax.fori_loop(
        0, STEPS, norm, ((zero,) * LANES, (zero,) * LANES)
    )
    stat_out[1, 0] = packed(first_b)
    stat_out[1, 1] = packed(second_b)
    for l in range(LANES):
        parts[l, 8 * KERNEL : 8 * KERNEL + 8] = by_gain[l]
        spare[8 * l : 8 * l + 8] = by_shift[l]
    phase("pair1")
    one, two = of_pair(1)
    phase("spread1")
    spread(one / width, first_b)
    spread(two / width, second_b)

    def folded(ref, start):
        rows = ref[pl.ds(start, 8, stride=8)]
        for s in range(1, SUB):
            rows = rows + ref[pl.ds(start + s, 8, stride=8)]
        return rows

    def to_axis(buffer, axis, places, index):
        own = buffer.at[places[0]]
        for device in along(axis, places):
            exchange(own, own, sh_send.at[index], sh_recv.at[index], device).start()

    def arrived(buffer, count, send, recv):
        if count > 1:
            some = buffer.at[pl.ds(0, count - 1)]
            pltpu.make_async_copy(some, some, recv).wait()
            pltpu.make_async_copy(some, some, send).wait()

    def from_axis(buffer, count, index):
        arrived(buffer, count, sh_send.at[index], sh_recv.at[index])
        result = buffer[0]
        for i in range(1, count):
            result = result + buffer[i]
        return result

    phase("gradconv")
    shift_x[x] = folded(spare, 0)
    to_axis(shift_x, "sp_2", xs, 0)

    @pl.loop(0, STEPS)
    def _(j):
        inv, one, two = inv_b[at_row(j)], first_b[at_row(j)], second_b[at_row(j)]
        for l in range(LANES):
            v = inv * (grad[l, at_row(j)] - one - conv[l, at_row(j)] * two)
            grad[l, at_row(j)] = v
            wide[l, pl.ds(PITCH + 16 + j, SUB, stride=PITCH)] = v
            wide[l, pl.ds(j + 48 + 80 * (j // 16), SUB, stride=PITCH)] = v

    for l in range(LANES):
        tail_out[0, l] = wide[l, 48:64]
        tail_out[1, l] = wide[l, 9 * PITCH : 9 * PITCH + 16]

    tails = [
        exchange(tail_out.at[0], tail_in.at[1], tail_send.at[0], tail_recv.at[1], before),
        exchange(tail_out.at[1], tail_in.at[0], tail_send.at[1], tail_recv.at[0], after),
    ]
    for copy in tails:
        copy.start()

    def send_tile(g, l, device_x, device_y):
        q = g * LANES + l
        exchange(
            tiles.at[q], tiles_in.at[mine], rs_send, rs_recv, {"sp_1": device_y, "sp_2": device_x}
        ).start()

    def lane_block(i):
        odd = lax.rem(i, 2)
        offset = LANES // 2 + (i // 2) * (1 - odd) - ((i + 1) // 2) * odd
        return lax.rem(y + offset, LANES)

    phase("taps")

    @pl.loop(0, LANES)
    def _(i):
        l = lane_block(i)
        for k0 in range(0, KERNEL, GROUP):
            count = min(GROUP, KERNEL - k0)
            sums = [zero] * count
            window = [
                gated[l, pl.ds(PITCH + 1 + k0 + n, SUB, stride=PITCH)]
                for n in range(STEPS + count - 1)
            ]
            for j in range(STEPS):
                g = grad[l, pl.ds(8 * j, 8)]
                for n in range(count):
                    sums[n] = sums[n] + g * window[j + n]
            for n in range(count):
                parts[l, pl.ds(8 * (k0 + n), 8)] = sums[n]
        for g in range(4):
            tiles[g * LANES + l] = folded(parts.at[l], 64 * g)

        @pl.when(i > 0)
        def _():
            done = lane_block(i - 1)
            for step in (2, 1, 3, 0):
                send_tile(xs[step], done, xs[step], done)

    phase("rs_start")
    for step in far_first(nx):
        send_tile(xs[step], y, xs[step], y)
    shift_y[y] = from_axis(shift_x, nx, 0)
    to_axis(shift_y, "sp_1", ys, 1)

    phase("tails")
    for copy in tails:
        copy.wait()
    for i in range(2):
        for l in range(LANES):
            wide[l, pl.ds(starts[i], 16)] = jnp.where(absent[i], 0.0, tail_in[i, l])

    phase("back")
    @pl.loop(0, LANES)
    def _(l):
        for j0 in range(0, STEPS, GROUP):
            low = PITCH + 31 - (KERNEL - 1) + j0
            window = [
                wide[l, pl.ds(low + i, SUB, stride=PITCH)] for i in range(GROUP + KERNEL - 1)
            ]
            sums = [zero] * GROUP
            for k in range(KERNEL):
                weight = tap(k, l)
                for i in range(GROUP):
                    sums[i] = sums[i] + weight * window[i + KERNEL - 1 - k]
            for i in range(GROUP):
                back[l, pl.ds(j0 + i, SUB, stride=OUT_PITCH)] = sums[i]

    @pl.loop(0, SUB)
    def _(s):
        for half in range(2):
            rows = pl.ds(pl.multiple_of(32 * s + 16 * half, 16), 16)
            for l in range(LANES):
                lanes = slice(128 * l, 128 * l + 128)
                g = back[l, pl.ds(pl.multiple_of(OUT_PITCH * s + 16 * half, 8), 16)]
                sig = sigmoid(gate[rows, lanes].astype(F32))
                d_value[rows, lanes] = (g * sig).astype(BF16)
                d_gate[rows, lanes] = (
                    g * value[rows, lanes].astype(F32) * sig * (1.0 - sig)
                ).astype(BF16)

    phase("rs_wait")
    scale = 1.0 / math.sqrt(total)
    arrived(tiles_in, plane, rs_send, rs_recv)
    line_own = tiles[mine]
    phase("rs_sum")
    tiles_in[mine] = line_own
    halves = [tiles_in[0], tiles_in[1]]
    for i in range(2, plane):
        halves[i % 2] = halves[i % 2] + tiles_in[i]
    line[z] = halves[0] + halves[1]

    for device in along("sp_0", zs):
        exchange(line.at[z], line.at[z], z_send, z_recv, device).start()
    shift_z[z] = from_axis(shift_y, ny, 1)
    to_axis(shift_z, "sp_0", zs, 2)


    phase("z_wait")
    arrived(line, nz, z_send, z_recv)
    phase("ag_start")
    result = line[0]
    for i in range(1, nz):
        result = result + line[i]
    final[mine] = result * scale

    for device in in_plane:
        exchange(final.at[mine], final.at[mine], ag_send, ag_recv, device).start()
    d_shift[...] = from_axis(shift_z, nz, 2) * scale

    phase("ag_wait")
    arrived(final, plane, ag_send, ag_recv)
    phase("finish")
    for g in range(4):
        for l in range(LANES):
            lanes = slice(128 * l, 128 * l + 128)
            if g < 3:
                d_taps[8 * g : 8 * g + 8, lanes] = final[g * LANES + l]
            else:
                last = final[g * LANES + l]
                d_taps[24:KERNEL, lanes] = last[:7]
                d_gain[:, lanes] = last[7:]
    phase(None)


def shards(dims, total, value_in, gate_in, taps, gain, shift, w_out, grad_out):
    nz, ny, nx = dims
    depth = grad_out.shape[1]
    vmem = pltpu.VMEM
    dma = pltpu.SemaphoreType.DMA
    padded = (LANES, 10 * PITCH, 128)
    rows = (LANES, ROWS, 128)
    spread = (LANES, SUB * OUT_PITCH, 128)
    scratch = [
        vmem((ROWS, WIDTH), BF16), vmem((ROWS, WIDTH), BF16), vmem((KERNEL, WIDTH), F32),
        vmem((1, WIDTH), F32), vmem((1, WIDTH), F32), vmem((WIDTH, depth), BF16),
        vmem((ROWS, depth), BF16),
        vmem(padded, F32), vmem(rows, F32), vmem(spread, F32), vmem(rows, F32),
        vmem(padded, F32), vmem(spread, F32), vmem(rows, F32), vmem((8, 128), F32),
        vmem((2, 16, WIDTH), BF16), vmem((2, 16, WIDTH), BF16), vmem((LANES, 48, 128), F32),
        vmem((2, LANES, 16, 128), F32), vmem((2, LANES, 16, 128), F32),
        vmem((2, 2, SUB, 128), F32), vmem((2, 2, SUB, 128), F32),
        vmem((ROWS, 128), F32), vmem((ROWS, 128), F32), vmem((ROWS, 128), F32),
        vmem((ROWS, 128), F32),
        vmem((32, 8, 128), F32), vmem((32, 8, 128), F32), vmem((nz, 8, 128), F32),
        vmem((32, 8, 128), F32), vmem((nx, 8, 128), F32), vmem((ny, 8, 128), F32),
        vmem((nz, 8, 128), F32), vmem((64, 128), F32),
        dma((6,)), dma((4,)), dma((2,)), dma((2,)), dma((2,)), dma((2,)), dma((2,)), dma((2,)),
        dma, dma, dma, dma, dma, dma, dma((3,)), dma((3,)),
    ]
    hbm = pl.BlockSpec(memory_space=pltpu.HBM)
    near = pl.BlockSpec(memory_space=pltpu.VMEM)
    shape = jax.ShapeDtypeStruct
    shapes = (
        shape((ROWS, WIDTH), BF16), shape((ROWS, WIDTH), BF16), shape((KERNEL, WIDTH), F32),
        shape((1, WIDTH), F32), shape((8, 128), F32),
    )
    results = pl.pallas_call(
        functools.partial(kernel, dims, total),
        out_shape=shapes,
        in_specs=[hbm] * 7,
        out_specs=(near,) * 5,
        scratch_shapes=scratch,
        compiler_params=pltpu.CompilerParams(
            collective_id=0, has_side_effects=True, vmem_limit_bytes=40 * 2**20
        ),
        name="module",
    )(*(pltpu.with_memory_space_constraint(a, pltpu.HBM) for a in (value_in, gate_in, taps, gain.reshape(1, WIDTH), shift.reshape(1, WIDTH), w_out, grad_out)))
    d_value, d_gate, d_taps, d_gain, d_shift = pl.pallas_call(
        put_out,
        out_shape=shapes,
        in_specs=[pl.BlockSpec(memory_space=pl.ANY)] * 5,
        out_specs=(hbm,) * 5,
        scratch_shapes=[dma((5,))],
        compiler_params=pltpu.CompilerParams(vmem_limit_bytes=2**20),
        name="put_out",
    )(*results)
    return d_value, d_gate, d_taps, d_gain.reshape(WIDTH), d_shift.reshape(WIDTH)


def put_out(*refs):
    sems = refs[10]
    copies = [pltpu.make_async_copy(refs[i], refs[5 + i], sems.at[i]) for i in range(5)]
    for copy in copies:
        copy.start()
    for copy in copies:
        copy.wait()


def solution(mesh, dims=(12, 8, 4)):
    finer = Mesh(mesh.devices.reshape(*dims, mesh.shape["tp"]), (*SP, "tp"))
    total = ROWS * math.prod(dims)
    return jax.shard_map(
        functools.partial(shards, dims, total),
        mesh=finer,
        in_specs=(
            P(SP, "tp"), P(SP, "tp"), P(None, "tp"), P("tp"), P("tp"), P("tp", None), P(SP, None),
        ),
        out_specs=(P(SP, "tp"), P(SP, "tp"), P(None, "tp"), P("tp"), P("tp")),
        check_vma=False,
    )
```

time: 72.3 us -> 51.6 us (0.71)
  Pallas kernels: 62.3 us -> 50.9 us
  local copies, waits for them, and re-layouts: 9.01 us -> 0 us
    pallas_call x1 -> x2, Pallas kernels: 62.3 us -> 50.9 us  [the longest x1 49.8 us: shards(): pl.pallas_call(functools.partial(kernel, dims, total), out_shape=shapes,...]
    unnamed x17 -> x0, local copies, waits for them, and re-layouts: 9.01 us -> none
where the time goes in v2:
time: 51.6 us; the launch traced here: 51.5 us
  Pallas kernels  50.9 us (99%)
  between operations  0.64 us (1%)
    pallas_call x1, Pallas kernels, shards(): pl.pallas_call(functools.partial(kernel, dims, total), out_shape=shapes,...  49.8 us
    pallas_call x1, Pallas kernels, shards(): pl.pallas_call(put_out, out_shape=shapes, in_specs=[pl.BlockSpec(memory_s...  1.05 us

profile of v2, /device:TPU:8, one launch (start us, length us, event | category | flops | bytes accessed | tf_op | source)
XLA Modules:
  0.0 51.5 jit_solution(3952151823202806803)
XLA Ops:
  0.6 49.8 %module.1 = (bf16[256,1024]{1,0:T(8,128)(2,1)S(1)}, bf16[256,1024]{1,0:T(8,128)(2,1)S(1)}, f32[31,1024]{1,0:T(8,128)S(1)}, f32[1,1024]{1,0:T(1,128)S(1)}, f32[8,128]{1,0:T(8,128)S(1)}) custom-call(bf16[256,1024]{1,0:T(8,128)(2,1)} %value_hbm.1, bf16[256,1024]{1,0:T(8,128)(2,1)} %gate_hbm.1, f32[31,1024]{1,0:T(8,128)} %taps_hbm.1, f32[1,1024]{1,0:T(1,128)} %bitcast.4, ...), custom_call_target="tpu_custom_call" | custom-call | tf_op jit(solution)/shard_map/module/pallas_call | solution.py:522
  50.5 1.1 %put_out.1 = (bf16[256,1024]{1,0:T(8,128)(2,1)}, bf16[256,1024]{1,0:T(8,128)(2,1)}, f32[31,1024]{1,0:T(8,128)}, f32[1,1024]{1,0:T(1,128)}, f32[8,128]{1,0:T(8,128)}) custom-call(bf16[256,1024]{1,0:T(8,128)(2,1)S(1)} %get-tuple-element.15.refs_0_, bf16[256,1024]{1,0:T(8,128)(2,1)S(1)} %get-tuple-element.16.refs_1_, f32[31,1024]{1,0:T(8,128)S(1)} %get-tuple-element.17.refs_2_, ...), custom_call_target="tpu_custom_call" | custom-call | tf_op jit(solution)/shard_map/put_out/pallas_call | solution.py:533

commit v3 on v2

--- a/solution.py
+++ b/solution.py
@@ -16,6 +16,8 @@
 MESH = pl.DeviceIdType.MESH
 
 ROWS, WIDTH, KERNEL, HALF = 256, 1024, 31, 15
+ADDER = 1
+ROUNDS = 6
 LANES, SUB, STEPS, PITCH, OUT_PITCH = 8, 8, 32, 72, 40
 GROUP = 8
 
@@ -54,11 +56,11 @@
     d_value, d_gate, d_taps, d_gain, d_shift,
     value, gate, taps, gain, shift, w, cot,
     gated, conv, mix, grad, wide, back, parts, bits,
-    edge_out, edge_in, edge, tail_out, tail_in,
+    edge_out, edge_in, edge, tail_out, tail_in, tail,
     stat_out, stat_in, mean_b, inv_b, first_b, second_b,
-    tiles, tiles_in, line, final, shift_x, shift_y, shift_z, spare,
+    tiles, tiles_in, line, final, other, shift_x, shift_y, shift_z, spare,
     in_sem, w_sem, edge_send, edge_recv, stat_send, stat_recv, tail_send, tail_recv,
-    rs_send, rs_recv, z_send, z_recv, ag_send, ag_recv, sh_send, sh_recv,
+    rs_send, rs_recv, z_send, z_recv, ag_send, ag_recv, sh_send, sh_recv, rounds,
 ):
     nz, ny, nx = dims
     z, y, x, t, me = position(dims)
@@ -102,13 +104,8 @@
         )
         for i in range(4)
     ]
-    small[0].start()
-    small[1].start()
-    small[5].start()
-    for copy in big:
+    for copy in small + big:
         copy.start()
-    for i in (2, 3, 4):
-        small[i].start()
 
     phase("greet")
     barrier = pltpu.get_barrier_semaphore()
@@ -116,8 +113,28 @@
     def greet(device):
         pl.semaphore_signal(barrier, inc=1, device_id=device, device_id_type=MESH)
 
-    for device in along("sp_0", zs) + in_plane + [after, before, partner]:
+    def core(device, which):
+        return {**device, "tp": which}
+
+    beside = [
+        {axis: places[step]}
+        for axis, places in (("sp_2", xs), ("sp_1", ys), ("sp_0", zs))
+        for step in (1, -1)
+        if len(places) > 1
+    ]
+    for device in [after, before, partner] + beside:
         greet(device)
+
+    def tell(turn):
+        for device in beside:
+            pl.semaphore_signal(
+                rounds.at[turn], inc=1, device_id=device, device_id_type=MESH
+            )
+
+    def hear(turn):
+        pl.semaphore_wait(rounds.at[turn], len(beside))
+        if turn + 1 < ROUNDS:
+            tell(turn + 1)
 
     phase("load")
     small[0].wait()
@@ -135,7 +152,9 @@
     for l in range(LANES):
         for start in starts:
             gated[l, pl.ds(start, 16)] = jnp.zeros((16, 128), F32)
+            wide[l, pl.ds(start, 16)] = jnp.zeros((16, 128), F32)
         edge[l, 16:32] = jnp.zeros((16, 128), F32)
+        tail[l, 16:32] = jnp.zeros((16, 128), F32)
 
     @pl.loop(0, SUB)
     def _(s):
@@ -148,9 +167,14 @@
                 other = pl.multiple_of(PITCH * s + 48 if half == 0 else PITCH * (s + 2), 8)
                 gated[l, pl.ds(other, 16)] = v
 
-    phase("project")
-    small[5].wait()
-    for i in range(4):
+    for i in (2, 3, 4):
+        small[i].wait()
+
+    def tap(k, l):
+        lanes = pl.ds(pl.multiple_of(128 * l, 128), 128)
+        return jnp.broadcast_to(taps[pl.ds(k, 1), lanes], (SUB, 128))
+
+    def project(i):
         big[i].wait()
         product = lax.dot_general(
             cot[...], w[pl.ds(256 * i, 256)], (((1,), (1,)), ((), ())),
@@ -162,32 +186,8 @@
                     32 * s : 32 * s + 32, 128 * part : 128 * part + 128
                 ]
 
-    for i in (2, 3, 4):
-        small[i].wait()
-
-    phase("barrier")
-    pl.semaphore_wait(barrier, (nz - 1) + (plane - 1) + 3)
-
-    def exchange(source, target, send, recv, device):
-        return pltpu.make_async_remote_copy(
-            src_ref=source, dst_ref=target, send_sem=send, recv_sem=recv,
-            device_id=device, device_id_type=MESH,
-        )
-
-    phase("edges")
-    edges = [
-        exchange(edge_out.at[0], edge_in.at[1], edge_send.at[0], edge_recv.at[1], before),
-        exchange(edge_out.at[1], edge_in.at[0], edge_send.at[1], edge_recv.at[0], after),
-    ]
-    for copy in edges:
-        copy.start()
-    def tap(k, l):
-        lanes = pl.ds(pl.multiple_of(128 * l, 128), 128)
-        return jnp.broadcast_to(taps[pl.ds(k, 1), lanes], (SUB, 128))
-
     phase("conv")
-    @pl.loop(0, LANES)
-    def _(l):
+    def convolve(l):
         for j0 in range(0, STEPS, GROUP):
             window = [
                 gated[l, pl.ds(PITCH + j0 + 1 + i, SUB, stride=PITCH)]
@@ -200,6 +200,37 @@
                     sums[i] = sums[i] + weight * window[i + k]
             for i in range(GROUP):
                 conv[l, pl.ds(8 * (j0 + i), 8)] = sums[i]
+
+    pl.loop(0, LANES // 2)(convolve)
+
+    phase("barrier")
+    pl.semaphore_wait(barrier, 3 + len(beside))
+    tell(0)
+
+    def exchange(source, target, send, recv, device):
+        return pltpu.make_async_remote_copy(
+            src_ref=source, dst_ref=target, send_sem=send, recv_sem=recv,
+            device_id=device, device_id_type=MESH,
+        )
+
+    phase("edges")
+    edges = [
+        exchange(edge_out.at[0], edge_in.at[1], edge_send.at[0], edge_recv.at[1], before),
+        exchange(edge_out.at[1], edge_in.at[0], edge_send.at[1], edge_recv.at[0], after),
+    ]
+    for copy in edges:
+        copy.start()
+    phase("conv2")
+    pl.loop(LANES // 2, LANES)(convolve)
+    hear(0)
+
+    phase("project")
+    small[5].wait()
+    project(0)
+    project(1)
+    hear(1)
+    project(2)
+    hear(2)
 
     phase("edges_wait")
     for copy in edges:
@@ -240,11 +271,14 @@
             result = jnp.where(lane == j, row, result)
         return result
 
-    def of_pair(slot):
+    def to_pair(slot):
         copy = exchange(
             stat_out.at[slot], stat_in.at[slot], stat_send.at[slot], stat_recv.at[slot], partner
         )
         copy.start()
+        return copy
+
+    def of_pair(copy, slot):
         copy.wait()
         return (
             stat_out[slot, 0] + stat_in[slot, 0],
@@ -270,7 +304,11 @@
     stat_out[0, 0] = packed(first_b)
     stat_out[0, 1] = packed(second_b)
     phase("pair0")
-    one, two = of_pair(0)
+    copy = to_pair(0)
+    hear(3)
+    project(3)
+    phase("pair0_wait")
+    one, two = of_pair(copy, 0)
     phase("spread0")
     width = 2.0 * WIDTH
     mean = one / width
@@ -306,11 +344,13 @@
     )
     stat_out[1, 0] = packed(first_b)
     stat_out[1, 1] = packed(second_b)
+    phase("pair1")
+    copy = to_pair(1)
+    hear(4)
     for l in range(LANES):
         parts[l, 8 * KERNEL : 8 * KERNEL + 8] = by_gain[l]
         spare[8 * l : 8 * l + 8] = by_shift[l]
-    phase("pair1")
-    one, two = of_pair(1)
+    one, two = of_pair(copy, 1)
     phase("spread1")
     spread(one / width, first_b)
     spread(two / width, second_b)
@@ -366,7 +406,8 @@
     def send_tile(g, l, device_x, device_y):
         q = g * LANES + l
         exchange(
-            tiles.at[q], tiles_in.at[mine], rs_send, rs_recv, {"sp_1": device_y, "sp_2": device_x}
+            tiles.at[q], tiles_in.at[t * plane + mine], rs_send, rs_recv,
+            {"sp_1": device_y, "sp_2": device_x, "tp": ADDER},
         ).start()
 
     def lane_block(i):
@@ -374,6 +415,7 @@
         offset = LANES // 2 + (i // 2) * (1 - odd) - ((i + 1) // 2) * odd
         return lax.rem(y + offset, LANES)
 
+    hear(5)
     phase("taps")
 
     @pl.loop(0, LANES)
@@ -404,15 +446,13 @@
     phase("rs_start")
     for step in far_first(nx):
         send_tile(xs[step], y, xs[step], y)
+
+    @pl.when(t != ADDER)
+    def _():
+        send_tile(x, y, x, y)
+
     shift_y[y] = from_axis(shift_x, nx, 0)
     to_axis(shift_y, "sp_1", ys, 1)
-
-    phase("tails")
-    for copy in tails:
-        copy.wait()
-    for i in range(2):
-        for l in range(LANES):
-            wide[l, pl.ds(starts[i], 16)] = jnp.where(absent[i], 0.0, tail_in[i, l])
 
     phase("back")
     @pl.loop(0, LANES)
@@ -430,6 +470,51 @@
             for i in range(GROUP):
                 back[l, pl.ds(j0 + i, SUB, stride=OUT_PITCH)] = sums[i]
 
+    def taken(sem, count):
+        some = tiles_in.at[pl.ds(0, count)]
+        pltpu.make_async_copy(some, some, sem).wait()
+
+    phase("rs_wait")
+
+    @pl.when(t == ADDER)
+    def _():
+        taken(rs_recv, 2 * plane - 1)
+        tiles_in[ADDER * plane + mine] = tiles[mine]
+        for which in range(2):
+            halves = [tiles_in[which * plane], tiles_in[which * plane + 1]]
+            for i in range(2, plane):
+                halves[i % 2] = halves[i % 2] + tiles_in[which * plane + i]
+            line[z, which] = halves[0] + halves[1]
+        for device in along("sp_0", zs):
+            exchange(line.at[z], line.at[z], z_send, z_recv, device).start()
+
+    phase("shift_z")
+    shift_z[z] = from_axis(shift_y, ny, 1)
+    to_axis(shift_z, "sp_0", zs, 2)
+
+    phase("tails")
+    for copy in tails:
+        copy.wait()
+    for i in range(2):
+        for l in range(LANES):
+            tail[l, pl.ds(32 * i, 16)] = jnp.where(absent[i], 0.0, tail_in[i, l])
+
+    @pl.loop(0, LANES)
+    def _(l):
+        for t0 in (0, 8):
+            low = zero
+            for k in range(16 + t0, KERNEL):
+                low = low + tap(k, l) * tail[l, pl.ds(31 + t0 - k, 8)]
+            rows = pl.ds(t0, 8)
+            back[l, rows] = back[l, rows] + low
+            high = zero
+            for k in range(7 + t0):
+                high = high + tap(k, l) * tail[l, pl.ds(31 + t0 - k, 8)]
+            rows = pl.ds(OUT_PITCH * 7 + 16 + t0, 8)
+            back[l, rows] = back[l, rows] + high
+
+    phase("outputs")
+
     @pl.loop(0, SUB)
     def _(s):
         for half in range(2):
@@ -445,35 +530,38 @@
 
     phase("rs_wait")
     scale = 1.0 / math.sqrt(total)
-    arrived(tiles_in, plane, rs_send, rs_recv)
-    line_own = tiles[mine]
-    phase("rs_sum")
-    tiles_in[mine] = line_own
-    halves = [tiles_in[0], tiles_in[1]]
-    for i in range(2, plane):
-        halves[i % 2] = halves[i % 2] + tiles_in[i]
-    line[z] = halves[0] + halves[1]
-
-    for device in along("sp_0", zs):
-        exchange(line.at[z], line.at[z], z_send, z_recv, device).start()
-    shift_z[z] = from_axis(shift_y, ny, 1)
-    to_axis(shift_z, "sp_0", zs, 2)
-
-
     phase("z_wait")
-    arrived(line, nz, z_send, z_recv)
-    phase("ag_start")
-    result = line[0]
-    for i in range(1, nz):
-        result = result + line[i]
-    final[mine] = result * scale
-
-    for device in in_plane:
-        exchange(final.at[mine], final.at[mine], ag_send, ag_recv, device).start()
+
+    @pl.when(t == ADDER)
+    def _():
+        arrived(line, nz, z_send, z_recv)
+        one, two = line[0, 0], line[0, 1]
+        for i in range(1, nz):
+            one, two = one + line[i, 0], two + line[i, 1]
+        final[mine] = two * scale
+        other[...] = one * scale
+        for device in in_plane:
+            exchange(other, final.at[mine], ag_send, ag_recv, core(device, 1 - ADDER)).start()
+            exchange(
+                final.at[mine], final.at[mine], ag_send, ag_recv, core(device, ADDER)
+            ).start()
+        exchange(other, final.at[mine], ag_send, ag_recv, partner).start()
+
+    phase("shift_wait")
     d_shift[...] = from_axis(shift_z, nz, 2) * scale
-
     phase("ag_wait")
-    arrived(final, plane, ag_send, ag_recv)
+
+    @pl.when(t == ADDER)
+    def _():
+        taken(ag_recv, plane - 1)
+        taken(ag_send, 2 * plane - 1)
+        taken(rs_send, plane - 1)
+
+    @pl.when(t != ADDER)
+    def _():
+        taken(ag_recv, plane)
+        taken(rs_send, plane)
+
     phase("finish")
     for g in range(4):
         for l in range(LANES):
@@ -503,14 +591,16 @@
         vmem(padded, F32), vmem(spread, F32), vmem(rows, F32), vmem((8, 128), F32),
         vmem((2, 16, WIDTH), BF16), vmem((2, 16, WIDTH), BF16), vmem((LANES, 48, 128), F32),
         vmem((2, LANES, 16, 128), F32), vmem((2, LANES, 16, 128), F32),
+        vmem((LANES, 48, 128), F32),
         vmem((2, 2, SUB, 128), F32), vmem((2, 2, SUB, 128), F32),
         vmem((ROWS, 128), F32), vmem((ROWS, 128), F32), vmem((ROWS, 128), F32),
         vmem((ROWS, 128), F32),
-        vmem((32, 8, 128), F32), vmem((32, 8, 128), F32), vmem((nz, 8, 128), F32),
-        vmem((32, 8, 128), F32), vmem((nx, 8, 128), F32), vmem((ny, 8, 128), F32),
+        vmem((32, 8, 128), F32), vmem((64, 8, 128), F32), vmem((nz, 2, 8, 128), F32),
+        vmem((32, 8, 128), F32), vmem((8, 128), F32), vmem((nx, 8, 128), F32), vmem((ny, 8, 128), F32),
         vmem((nz, 8, 128), F32), vmem((64, 128), F32),
         dma((6,)), dma((4,)), dma((2,)), dma((2,)), dma((2,)), dma((2,)), dma((2,)), dma((2,)),
         dma, dma, dma, dma, dma, dma, dma((3,)), dma((3,)),
+        pltpu.SemaphoreType.REGULAR((ROUNDS,)),
     ]
     hbm = pl.BlockSpec(memory_space=pltpu.HBM)
     near = pl.BlockSpec(memory_space=pltpu.VMEM)

time: 51.6 us -> 52.1 us (level)
  the two profiles are of different devices: /device:TPU:8 before, /device:TPU:1 now
where the time goes in v3:
time: 52.1 us; the launch traced here: 51.9 us
  Pallas kernels  51.3 us (98%)
  between operations  0.64 us (1%)
    pallas_call x1, Pallas kernels, shards(): pl.pallas_call(functools.partial(kernel, dims, total), out_shape=shapes,...  50.2 us
    pallas_call x1, Pallas kernels, shards(): pl.pallas_call(put_out, out_shape=shapes, in_specs=[pl.BlockSpec(memory_s...  1.05 us

profile of v3, /device:TPU:1, one launch (start us, length us, event | category | flops | bytes accessed | tf_op | source)
XLA Modules:
  0.0 51.9 jit_solution(11671499008403485033)
XLA Ops:
  0.6 50.2 %module.1 = (bf16[256,1024]{1,0:T(8,128)(2,1)S(1)}, bf16[256,1024]{1,0:T(8,128)(2,1)S(1)}, f32[31,1024]{1,0:T(8,128)S(1)}, f32[1,1024]{1,0:T(1,128)S(1)}, f32[8,128]{1,0:T(8,128)S(1)}) custom-call(bf16[256,1024]{1,0:T(8,128)(2,1)} %value_hbm.1, bf16[256,1024]{1,0:T(8,128)(2,1)} %gate_hbm.1, f32[31,1024]{1,0:T(8,128)} %taps_hbm.1, f32[1,1024]{1,0:T(1,128)} %bitcast.4, ...), custom_call_target="tpu_custom_call" | custom-call | tf_op jit(solution)/shard_map/module/pallas_call | solution.py:612
  50.9 1.1 %put_out.1 = (bf16[256,1024]{1,0:T(8,128)(2,1)}, bf16[256,1024]{1,0:T(8,128)(2,1)}, f32[31,1024]{1,0:T(8,128)}, f32[1,1024]{1,0:T(1,128)}, f32[8,128]{1,0:T(8,128)}) custom-call(bf16[256,1024]{1,0:T(8,128)(2,1)S(1)} %get-tuple-element.15.refs_0_, bf16[256,1024]{1,0:T(8,128)(2,1)S(1)} %get-tuple-element.16.refs_1_, f32[31,1024]{1,0:T(8,128)S(1)} %get-tuple-element.17.refs_2_, ...), custom_call_target="tpu_custom_call" | custom-call | tf_op jit(solution)/shard_map/put_out/pallas_call | solution.py:623

commit v4 on v3

--- a/solution.py
+++ b/solution.py
@@ -17,7 +17,8 @@
 
 ROWS, WIDTH, KERNEL, HALF = 256, 1024, 31, 15
 ADDER = 1
-ROUNDS = 6
+REACH = (1, 2, 4)
+ROUNDS = len(REACH) + 1
 LANES, SUB, STEPS, PITCH, OUT_PITCH = 8, 8, 32, 72, 40
 GROUP = 8
 
@@ -116,23 +117,28 @@
     def core(device, which):
         return {**device, "tp": which}
 
-    beside = [
-        {axis: places[step]}
-        for axis, places in (("sp_2", xs), ("sp_1", ys), ("sp_0", zs))
-        for step in (1, -1)
-        if len(places) > 1
-    ]
-    for device in [after, before, partner] + beside:
+    def at_distance(reach):
+        found = []
+        for axis, places in (("sp_2", xs), ("sp_1", ys), ("sp_0", zs)):
+            count = len(places)
+            if count > reach:
+                found.append({axis: places[reach]})
+                if count - reach > reach:
+                    found.append({axis: places[-reach]})
+        return found
+
+    heard = [at_distance(reach) for reach in REACH] + [[partner]]
+    for device in [after, before, partner] + heard[0]:
         greet(device)
 
     def tell(turn):
-        for device in beside:
+        for device in heard[turn]:
             pl.semaphore_signal(
                 rounds.at[turn], inc=1, device_id=device, device_id_type=MESH
             )
 
     def hear(turn):
-        pl.semaphore_wait(rounds.at[turn], len(beside))
+        pl.semaphore_wait(rounds.at[turn], len(heard[turn]))
         if turn + 1 < ROUNDS:
             tell(turn + 1)
 
@@ -204,7 +210,7 @@
     pl.loop(0, LANES // 2)(convolve)
 
     phase("barrier")
-    pl.semaphore_wait(barrier, 3 + len(beside))
+    pl.semaphore_wait(barrier, 3 + len(heard[0]))
     tell(0)
 
     def exchange(source, target, send, recv, device):
@@ -226,11 +232,9 @@
 
     phase("project")
     small[5].wait()
-    project(0)
-    project(1)
+    for i in range(3):
+        project(i)
     hear(1)
-    project(2)
-    hear(2)
 
     phase("edges_wait")
     for copy in edges:
@@ -305,7 +309,6 @@
     stat_out[0, 1] = packed(second_b)
     phase("pair0")
     copy = to_pair(0)
-    hear(3)
     project(3)
     phase("pair0_wait")
     one, two = of_pair(copy, 0)
@@ -346,7 +349,7 @@
     stat_out[1, 1] = packed(second_b)
     phase("pair1")
     copy = to_pair(1)
-    hear(4)
+    hear(2)
     for l in range(LANES):
         parts[l, 8 * KERNEL : 8 * KERNEL + 8] = by_gain[l]
         spare[8 * l : 8 * l + 8] = by_shift[l]
@@ -379,29 +382,9 @@
             result = result + buffer[i]
         return result
 
-    phase("gradconv")
+    phase("shift_x")
     shift_x[x] = folded(spare, 0)
     to_axis(shift_x, "sp_2", xs, 0)
-
-    @pl.loop(0, STEPS)
-    def _(j):
-        inv, one, two = inv_b[at_row(j)], first_b[at_row(j)], second_b[at_row(j)]
-        for l in range(LANES):
-            v = inv * (grad[l, at_row(j)] - one - conv[l, at_row(j)] * two)
-            grad[l, at_row(j)] = v
-            wide[l, pl.ds(PITCH + 16 + j, SUB, stride=PITCH)] = v
-            wide[l, pl.ds(j + 48 + 80 * (j // 16), SUB, stride=PITCH)] = v
-
-    for l in range(LANES):
-        tail_out[0, l] = wide[l, 48:64]
-        tail_out[1, l] = wide[l, 9 * PITCH : 9 * PITCH + 16]
-
-    tails = [
-        exchange(tail_out.at[0], tail_in.at[1], tail_send.at[0], tail_recv.at[1], before),
-        exchange(tail_out.at[1], tail_in.at[0], tail_send.at[1], tail_recv.at[0], after),
-    ]
-    for copy in tails:
-        copy.start()
 
     def send_tile(g, l, device_x, device_y):
         q = g * LANES + l
@@ -415,12 +398,18 @@
         offset = LANES // 2 + (i // 2) * (1 - odd) - ((i + 1) // 2) * odd
         return lax.rem(y + offset, LANES)
 
-    hear(5)
+    hear(3)
     phase("taps")
 
     @pl.loop(0, LANES)
     def _(i):
         l = lane_block(i)
+        for j in range(STEPS):
+            rows = pl.ds(8 * j, 8)
+            v = inv_b[rows] * (grad[l, rows] - first_b[rows] - conv[l, rows] * second_b[rows])
+            grad[l, rows] = v
+            wide[l, pl.ds(PITCH + 16 + j, SUB, stride=PITCH)] = v
+            wide[l, pl.ds(j + 48 + 80 * (j // 16), SUB, stride=PITCH)] = v
         for k0 in range(0, KERNEL, GROUP):
             count = min(GROUP, KERNEL - k0)
             sums = [zero] * count
@@ -451,8 +440,17 @@
     def _():
         send_tile(x, y, x, y)
 
+    for l in range(LANES):
+        tail_out[0, l] = wide[l, 48:64]
+        tail_out[1, l] = wide[l, 9 * PITCH : 9 * PITCH + 16]
     shift_y[y] = from_axis(shift_x, nx, 0)
     to_axis(shift_y, "sp_1", ys, 1)
+    tails = [
+        exchange(tail_out.at[0], tail_in.at[1], tail_send.at[0], tail_recv.at[1], before),
+        exchange(tail_out.at[1], tail_in.at[0], tail_send.at[1], tail_recv.at[0], after),
+    ]
+    for copy in tails:
+        copy.start()
 
     phase("back")
     @pl.loop(0, LANES)

time: 52.1 us -> 49.4 us (0.948)
  Pallas kernels: 51.3 us -> 48.6 us
    pallas_call x1, Pallas kernels: 50.2 us -> 47.6 us  [shards(): pl.pallas_call(functools.partial(kernel, dims, total), out_shape=shapes,...]
where the time goes in v4:
time: 49.4 us; the launch traced here: 49.3 us
  Pallas kernels  48.6 us (98%)
  between operations  0.64 us (1%)
    pallas_call x1, Pallas kernels, shards(): pl.pallas_call(functools.partial(kernel, dims, total), out_shape=shapes,...  47.6 us
    pallas_call x1, Pallas kernels, shards(): pl.pallas_call(put_out, out_shape=shapes, in_specs=[pl.BlockSpec(memory_s...  1.05 us

profile of v4, /device:TPU:1, one launch (start us, length us, event | category | flops | bytes accessed | tf_op | source)
XLA Modules:
  0.0 49.3 jit_solution(11600212943250932184)
XLA Ops:
  0.6 47.6 %module.1 = (bf16[256,1024]{1,0:T(8,128)(2,1)S(1)}, bf16[256,1024]{1,0:T(8,128)(2,1)S(1)}, f32[31,1024]{1,0:T(8,128)S(1)}, f32[1,1024]{1,0:T(1,128)S(1)}, f32[8,128]{1,0:T(8,128)S(1)}) custom-call(bf16[256,1024]{1,0:T(8,128)(2,1)} %value_hbm.1, bf16[256,1024]{1,0:T(8,128)(2,1)} %gate_hbm.1, f32[31,1024]{1,0:T(8,128)} %taps_hbm.1, f32[1,1024]{1,0:T(1,128)} %bitcast.4, ...), custom_call_target="tpu_custom_call" | custom-call | tf_op jit(solution)/shard_map/module/pallas_call | solution.py:610
  48.2 1.1 %put_out.1 = (bf16[256,1024]{1,0:T(8,128)(2,1)}, bf16[256,1024]{1,0:T(8,128)(2,1)}, f32[31,1024]{1,0:T(8,128)}, f32[1,1024]{1,0:T(1,128)}, f32[8,128]{1,0:T(8,128)}) custom-call(bf16[256,1024]{1,0:T(8,128)(2,1)S(1)} %get-tuple-element.15.refs_0_, bf16[256,1024]{1,0:T(8,128)(2,1)S(1)} %get-tuple-element.16.refs_1_, f32[31,1024]{1,0:T(8,128)S(1)} %get-tuple-element.17.refs_2_, ...), custom_call_target="tpu_custom_call" | custom-call | tf_op jit(solution)/shard_map/put_out/pallas_call | solution.py:621

commit v5 on v4

--- a/solution.py
+++ b/solution.py
@@ -20,7 +20,8 @@
 REACH = (1, 2, 4)
 ROUNDS = len(REACH) + 1
 LANES, SUB, STEPS, PITCH, OUT_PITCH = 8, 8, 32, 72, 40
-GROUP = 8
+GROUP = 16
+TAP_GROUP = 16
 
 
 def position(dims):
@@ -58,7 +59,7 @@
     value, gate, taps, gain, shift, w, cot,
     gated, conv, mix, grad, wide, back, parts, bits,
     edge_out, edge_in, edge, tail_out, tail_in, tail,
-    stat_out, stat_in, mean_b, inv_b, first_b, second_b,
+    stat_out, stat_in, mean_b, inv_b, first_b, second_b, even, odd,
     tiles, tiles_in, line, final, other, shift_x, shift_y, shift_z, spare,
     in_sem, w_sem, edge_send, edge_recv, stat_send, stat_recv, tail_send, tail_recv,
     rs_send, rs_recv, z_send, z_recv, ag_send, ag_recv, sh_send, sh_recv, rounds,
@@ -228,13 +229,13 @@
         copy.start()
     phase("conv2")
     pl.loop(LANES // 2, LANES)(convolve)
-    hear(0)
 
     phase("project")
     small[5].wait()
-    for i in range(3):
-        project(i)
-    hear(1)
+    project(0)
+    hear(0)
+    project(1)
+    project(2)
 
     phase("edges_wait")
     for copy in edges:
@@ -309,6 +310,7 @@
     stat_out[0, 1] = packed(second_b)
     phase("pair0")
     copy = to_pair(0)
+    hear(1)
     project(3)
     phase("pair0_wait")
     one, two = of_pair(copy, 0)
@@ -343,7 +345,7 @@
 
     phase("norm")
     by_gain, by_shift = lax.fori_loop(
-        0, STEPS, norm, ((zero,) * LANES, (zero,) * LANES)
+        0, STEPS, norm, ((zero,) * LANES, (zero,) * LANES), unroll=2
     )
     stat_out[1, 0] = packed(first_b)
     stat_out[1, 1] = packed(second_b)
@@ -401,36 +403,52 @@
     hear(3)
     phase("taps")
 
-    @pl.loop(0, LANES)
-    def _(i):
-        l = lane_block(i)
-        for j in range(STEPS):
+    def grad_conv(l, target, steps):
+        for j in steps:
             rows = pl.ds(8 * j, 8)
             v = inv_b[rows] * (grad[l, rows] - first_b[rows] - conv[l, rows] * second_b[rows])
-            grad[l, rows] = v
+            target[rows] = v
             wide[l, pl.ds(PITCH + 16 + j, SUB, stride=PITCH)] = v
             wide[l, pl.ds(j + 48 + 80 * (j // 16), SUB, stride=PITCH)] = v
-        for k0 in range(0, KERNEL, GROUP):
-            count = min(GROUP, KERNEL - k0)
+
+    def tap_sums(l, source, meanwhile):
+        for k0 in range(0, KERNEL, TAP_GROUP):
+            count = min(TAP_GROUP, KERNEL - k0)
             sums = [zero] * count
             window = [
                 gated[l, pl.ds(PITCH + 1 + k0 + n, SUB, stride=PITCH)]
                 for n in range(STEPS + count - 1)
             ]
             for j in range(STEPS):
-                g = grad[l, pl.ds(8 * j, 8)]
+                g = source[8 * j : 8 * j + 8]
                 for n in range(count):
                     sums[n] = sums[n] + g * window[j + n]
+                if j % 2:
+                    meanwhile(k0 + j // 2)
             for n in range(count):
                 parts[l, pl.ds(8 * (k0 + n), 8)] = sums[n]
         for g in range(4):
             tiles[g * LANES + l] = folded(parts.at[l], 64 * g)
 
-        @pl.when(i > 0)
-        def _():
-            done = lane_block(i - 1)
-            for step in (2, 1, 3, 0):
-                send_tile(xs[step], done, xs[step], done)
+    def send_tiles(l):
+        for step in (2, 1, 3, 0):
+            send_tile(xs[step], l, xs[step], l)
+
+    grad_conv(lane_block(0), even, range(STEPS))
+
+    @pl.loop(0, LANES // 2)
+    def _(pair):
+        for n, (now, then) in enumerate(((even, odd), (odd, even))):
+            i = 2 * pair + n
+            coming = lane_block(i + 1)
+            tap_sums(lane_block(i), now, lambda j: grad_conv(coming, then, [j]))
+            if n:
+                send_tiles(lane_block(i - 1))
+            else:
+
+                @pl.when(pair > 0)
+                def _():
+                    send_tiles(lane_block(i - 1))
 
     phase("rs_start")
     for step in far_first(nx):
@@ -592,7 +610,7 @@
         vmem((LANES, 48, 128), F32),
         vmem((2, 2, SUB, 128), F32), vmem((2, 2, SUB, 128), F32),
         vmem((ROWS, 128), F32), vmem((ROWS, 128), F32), vmem((ROWS, 128), F32),
-        vmem((ROWS, 128), F32),
+        vmem((ROWS, 128), F32), vmem((ROWS, 128), F32), vmem((ROWS, 128), F32),
         vmem((32, 8, 128), F32), vmem((64, 8, 128), F32), vmem((nz, 2, 8, 128), F32),
         vmem((32, 8, 128), F32), vmem((8, 128), F32), vmem((nx, 8, 128), F32), vmem((ny, 8, 128), F32),
         vmem((nz, 8, 128), F32), vmem((64, 128), F32),
@@ -623,7 +641,7 @@
         out_shape=shapes,
         in_specs=[pl.BlockSpec(memory_space=pl.ANY)] * 5,
         out_specs=(hbm,) * 5,
-        scratch_shapes=[dma((5,))],
+        scratch_shapes=[dma((11,))],
         compiler_params=pltpu.CompilerParams(vmem_limit_bytes=2**20),
         name="put_out",
     )(*results)
@@ -632,7 +650,12 @@
 
 def put_out(*refs):
     sems = refs[10]
-    copies = [pltpu.make_async_copy(refs[i], refs[5 + i], sems.at[i]) for i in range(5)]
+    pieces = [(i, pl.ds(64 * n, 64)) for n in range(4) for i in range(2)]
+    pieces += [(i, slice(None)) for i in range(2, 5)]
+    copies = [
+        pltpu.make_async_copy(refs[i].at[rows], refs[5 + i].at[rows], sems.at[n])
+        for n, (i, rows) in enumerate(pieces)
+    ]
     for copy in copies:
         copy.start()
     for copy in copies:

time: 49.4 us -> 49.9 us (1.010)
  Pallas kernels: 48.6 us -> 49.1 us
where the time goes in v5:
time: 49.9 us; the launch traced here: 49.7 us
  Pallas kernels  49.1 us (98%)
  between operations  0.64 us (1%)
    pallas_call x1, Pallas kernels, shards(): pl.pallas_call(functools.partial(kernel, dims, total), out_shape=shapes,...  48 us
    pallas_call x1, Pallas kernels, shards(): pl.pallas_call(put_out, out_shape=shapes, in_specs=[pl.BlockSpec(memory_s...  1.1 us

profile of v5, /device:TPU:1, one launch (start us, length us, event | category | flops | bytes accessed | tf_op | source)
XLA Modules:
  0.0 49.7 jit_solution(16681523524084805324)
XLA Ops:
  0.6 48.0 %module.1 = (bf16[256,1024]{1,0:T(8,128)(2,1)S(1)}, bf16[256,1024]{1,0:T(8,128)(2,1)S(1)}, f32[31,1024]{1,0:T(8,128)S(1)}, f32[1,1024]{1,0:T(1,128)S(1)}, f32[8,128]{1,0:T(8,128)S(1)}) custom-call(bf16[256,1024]{1,0:T(8,128)(2,1)} %value_hbm.1, bf16[256,1024]{1,0:T(8,128)(2,1)} %gate_hbm.1, f32[31,1024]{1,0:T(8,128)} %taps_hbm.1, f32[1,1024]{1,0:T(1,128)} %bitcast.4, ...), custom_call_target="tpu_custom_call" | custom-call | tf_op jit(solution)/shard_map/module/pallas_call | solution.py:628
  48.6 1.1 %put_out.1 = (bf16[256,1024]{1,0:T(8,128)(2,1)}, bf16[256,1024]{1,0:T(8,128)(2,1)}, f32[31,1024]{1,0:T(8,128)}, f32[1,1024]{1,0:T(1,128)}, f32[8,128]{1,0:T(8,128)}) custom-call(bf16[256,1024]{1,0:T(8,128)(2,1)S(1)} %get-tuple-element.15.refs_0_, bf16[256,1024]{1,0:T(8,128)(2,1)S(1)} %get-tuple-element.16.refs_1_, f32[31,1024]{1,0:T(8,128)S(1)} %get-tuple-element.17.refs_2_, ...), custom_call_target="tpu_custom_call" | custom-call | tf_op jit(solution)/shard_map/put_out/pallas_call | solution.py:639

commit v6 on v5

--- a/solution.py
+++ b/solution.py
@@ -236,6 +236,7 @@
     hear(0)
     project(1)
     project(2)
+    hear(1)
 
     phase("edges_wait")
     for copy in edges:
@@ -310,7 +311,6 @@
     stat_out[0, 1] = packed(second_b)
     phase("pair0")
     copy = to_pair(0)
-    hear(1)
     project(3)
     phase("pair0_wait")
     one, two = of_pair(copy, 0)
@@ -351,7 +351,6 @@
     stat_out[1, 1] = packed(second_b)
     phase("pair1")
     copy = to_pair(1)
-    hear(2)
     for l in range(LANES):
         parts[l, 8 * KERNEL : 8 * KERNEL + 8] = by_gain[l]
         spare[8 * l : 8 * l + 8] = by_shift[l]
@@ -400,7 +399,7 @@
         offset = LANES // 2 + (i // 2) * (1 - odd) - ((i + 1) // 2) * odd
         return lax.rem(y + offset, LANES)
 
-    hear(3)
+    hear(2)
     phase("taps")
 
     def grad_conv(l, target, steps):
@@ -443,6 +442,11 @@
             coming = lane_block(i + 1)
             tap_sums(lane_block(i), now, lambda j: grad_conv(coming, then, [j]))
             if n:
+
+                @pl.when(pair == 0)
+                def _():
+                    hear(3)
+
                 send_tiles(lane_block(i - 1))
             else:
 
@@ -641,7 +645,7 @@
         out_shape=shapes,
         in_specs=[pl.BlockSpec(memory_space=pl.ANY)] * 5,
         out_specs=(hbm,) * 5,
-        scratch_shapes=[dma((11,))],
+        scratch_shapes=[dma((5,))],
         compiler_params=pltpu.CompilerParams(vmem_limit_bytes=2**20),
         name="put_out",
     )(*results)
@@ -650,12 +654,7 @@
 
 def put_out(*refs):
     sems = refs[10]
-    pieces = [(i, pl.ds(64 * n, 64)) for n in range(4) for i in range(2)]
-    pieces += [(i, slice(None)) for i in range(2, 5)]
-    copies = [
-        pltpu.make_async_copy(refs[i].at[rows], refs[5 + i].at[rows], sems.at[n])
-        for n, (i, rows) in enumerate(pieces)
-    ]
+    copies = [pltpu.make_async_copy(refs[i], refs[5 + i], sems.at[i]) for i in range(5)]
     for copy in copies:
         copy.start()
     for copy in copies:

time: 49.9 us -> 49.1 us (0.984)
  Pallas kernels: 49.1 us -> 48.3 us
    pallas_call x1, Pallas kernels: 48 us -> 47.3 us  [shards(): pl.pallas_call(functools.partial(kernel, dims, total), out_shape=shapes,...]
where the time goes in v6:
time: 49.1 us; the launch traced here: 49 us
  Pallas kernels  48.3 us (98%)
  between operations  0.64 us (1%)
    pallas_call x1, Pallas kernels, shards(): pl.pallas_call(functools.partial(kernel, dims, total), out_shape=shapes,...  47.3 us
    pallas_call x1, Pallas kernels, shards(): pl.pallas_call(put_out, out_shape=shapes, in_specs=[pl.BlockSpec(memory_s...  1.05 us

profile of v6, /device:TPU:1, one launch (start us, length us, event | category | flops | bytes accessed | tf_op | source)
XLA Modules:
  0.0 49.0 jit_solution(15673730980650100487)
XLA Ops:
  0.6 47.3 %module.1 = (bf16[256,1024]{1,0:T(8,128)(2,1)S(1)}, bf16[256,1024]{1,0:T(8,128)(2,1)S(1)}, f32[31,1024]{1,0:T(8,128)S(1)}, f32[1,1024]{1,0:T(1,128)S(1)}, f32[8,128]{1,0:T(8,128)S(1)}) custom-call(bf16[256,1024]{1,0:T(8,128)(2,1)} %value_hbm.1, bf16[256,1024]{1,0:T(8,128)(2,1)} %gate_hbm.1, f32[31,1024]{1,0:T(8,128)} %taps_hbm.1, f32[1,1024]{1,0:T(1,128)} %bitcast.4, ...), custom_call_target="tpu_custom_call" | custom-call | tf_op jit(solution)/shard_map/module/pallas_call | solution.py:632
  47.9 1.1 %put_out.1 = (bf16[256,1024]{1,0:T(8,128)(2,1)}, bf16[256,1024]{1,0:T(8,128)(2,1)}, f32[31,1024]{1,0:T(8,128)}, f32[1,1024]{1,0:T(1,128)}, f32[8,128]{1,0:T(8,128)}) custom-call(bf16[256,1024]{1,0:T(8,128)(2,1)S(1)} %get-tuple-element.15.refs_0_, bf16[256,1024]{1,0:T(8,128)(2,1)S(1)} %get-tuple-element.16.refs_1_, f32[31,1024]{1,0:T(8,128)S(1)} %get-tuple-element.17.refs_2_, ...), custom_call_target="tpu_custom_call" | custom-call | tf_op jit(solution)/shard_map/put_out/pallas_call | solution.py:643

commit v7 on v6

--- a/solution.py
+++ b/solution.py
@@ -250,7 +250,7 @@
             gated[l, pl.ds(starts[i], 16)] = v
             edge[l, pl.ds(32 * i, 16)] = v
 
-    @pl.loop(0, LANES)
+    @pl.loop(0, LANES, unroll=2)
     def _(l):
         for t0 in (0, 8):
             low = jnp.zeros((SUB, 128), F32)
@@ -345,7 +345,7 @@
 
     phase("norm")
     by_gain, by_shift = lax.fori_loop(
-        0, STEPS, norm, ((zero,) * LANES, (zero,) * LANES), unroll=2
+        0, STEPS, norm, ((zero,) * LANES, (zero,) * LANES), unroll=4
     )
     stat_out[1, 0] = packed(first_b)
     stat_out[1, 1] = packed(second_b)

time: 49.1 us -> 49 us (level)
  no operation moved by 1% of the time
where the time goes in v7:
time: 49 us; the launch traced here: 48.8 us
  Pallas kernels  48.2 us (98%)
  between operations  0.64 us (1%)
    pallas_call x1, Pallas kernels, shards(): pl.pallas_call(functools.partial(kernel, dims, total), out_shape=shapes,...  47.1 us
    pallas_call x1, Pallas kernels, shards(): pl.pallas_call(put_out, out_shape=shapes, in_specs=[pl.BlockSpec(memory_s...  1.05 us

profile of v7, /device:TPU:1, one launch (start us, length us, event | category | flops | bytes accessed | tf_op | source)
XLA Modules:
  0.0 48.8 jit_solution(16784035832614471780)
XLA Ops:
  0.6 47.1 %module.1 = (bf16[256,1024]{1,0:T(8,128)(2,1)S(1)}, bf16[256,1024]{1,0:T(8,128)(2,1)S(1)}, f32[31,1024]{1,0:T(8,128)S(1)}, f32[1,1024]{1,0:T(1,128)S(1)}, f32[8,128]{1,0:T(8,128)S(1)}) custom-call(bf16[256,1024]{1,0:T(8,128)(2,1)} %value_hbm.1, bf16[256,1024]{1,0:T(8,128)(2,1)} %gate_hbm.1, f32[31,1024]{1,0:T(8,128)} %taps_hbm.1, f32[1,1024]{1,0:T(1,128)} %bitcast.4, ...), custom_call_target="tpu_custom_call" | custom-call | tf_op jit(solution)/shard_map/module/pallas_call | solution.py:632
  47.8 1.1 %put_out.1 = (bf16[256,1024]{1,0:T(8,128)(2,1)}, bf16[256,1024]{1,0:T(8,128)(2,1)}, f32[31,1024]{1,0:T(8,128)}, f32[1,1024]{1,0:T(1,128)}, f32[8,128]{1,0:T(8,128)}) custom-call(bf16[256,1024]{1,0:T(8,128)(2,1)S(1)} %get-tuple-element.15.refs_0_, bf16[256,1024]{1,0:T(8,128)(2,1)S(1)} %get-tuple-element.16.refs_1_, f32[31,1024]{1,0:T(8,128)S(1)} %get-tuple-element.17.refs_2_, ...), custom_call_target="tpu_custom_call" | custom-call | tf_op jit(solution)/shard_map/put_out/pallas_call | solution.py:643
